TPU v7x, 32 devices: a whole 2x2x4 slice. The times are simulated.
32 devices in a mesh: grp: 2 (over y), ep: 4 (over z), tp: 4 (over x, core).
Axes of the slice: x: 2, y: 2, z: 4, core: 2. Of those that a mesh axis runs over, the one named last changes fastest.
Arguments:
- queries: bfloat16 [4096, 1024], P(('grp', 'ep'), 'tp'), parts along dimension 0, may hold values from -6 to 6
- key_rows: bfloat16 [4096, 512], P(('grp', 'ep'), 'tp'), parts along dimension 0, may hold values from -6 to 6
- value_rows: bfloat16 [4096, 512], P(('grp', 'ep'), 'tp'), parts along dimension 0, may hold values from -6 to 6
- query_gain: float32 [128], replicated, may hold values from 0.3 to 9
- key_gain: float32 [128], replicated, may hold values from 0.3 to 9
- log_forget: float32 [8, 4096], P('tp', 'grp'), parts along dimension 1, may hold values from -2048 to 0, as said below
- out_weight: bfloat16 [1024, 2048], P('tp'), may hold values from -0.1875 to 0.1875
- expert_rows: bfloat16 [4096, 2048], P(('grp', 'ep')), parts along dimension 0, may hold values from -6 to 6
- expert_gain: float32 [2048], replicated, may hold values from 0.1 to 1.9
- routes: int32 [2, 4096], P(None, ('grp', 'ep')), parts along dimension 1, may hold values from 0 to 31, as said below
- route_weight: float32 [2, 4096], P(None, ('grp', 'ep')), parts along dimension 1, may hold values from 0.1 to 1
- gate_weight: bfloat16 [32, 2048, 1024], P('ep', None, 'tp'), may hold values from -0.125 to 0.125
- up_weight: bfloat16 [32, 2048, 1024], P('ep', None, 'tp'), may hold values from -0.125 to 0.125
- down_weight: bfloat16 [32, 1024, 2048], P('ep', 'tp'), may hold values from -0.1875 to 0.1875
Outputs:
- mixer_out: bfloat16 [4096, 2048], P(('grp', 'ep', 'tp')), parts along dimension 0
- expert_out: bfloat16 [4096, 2048], P(('grp', 'ep'), 'tp'), parts along dimension 0
There are 2 independent parts, one for each index of `grp`. A program takes and returns all parts, laid end to end along the dimension named above; an argument that names none is the same for every part. Nothing has to cross between parts.
Inputs may be any that keep to these rules, and one draw needn't show every extreme that they name: `log_forget`: each head's values never rise along the positions. `routes`: the 2 experts of a token differ and lie in one group of 8 consecutive numbers. Among the tokens of one index of ep (512 consecutive tokens), no expert is named more than 48 times, and in every draw some experts are named exactly 48 times in every such block.
All inputs are finite; a program needn't handle non-finite values.
Results may differ from a plain program's by a relative error of at most 0.012.
The roundings to bfloat16 on the way count: a program that leaves them out, or rounds other values in their place, can miss the bound.
Values may be sent and summed in bfloat16 or wider, within the bound.
A program may use at most 128 MiB of HBM per device.

v0:
```python
import functools

import jax
import jax.numpy as jnp
from jax import lax
from jax.experimental import pallas as pl
from jax.experimental.pallas import tpu as pltpu
from jax.sharding import PartitionSpec as P

HEAD_SIZE = 128
EXPERTS = 32
TOP = 2
GROUP_SIZE = 8
META = 128


def head_norm(inputs, scale_gain):
    widened = inputs.astype(jnp.float32)
    factor = lax.rsqrt(jnp.mean(widened * widened, axis=-1, keepdims=True) + 1e-06)
    return widened * factor * scale_gain


def slot_table(chosen, experts_all, capacity):
    n_rows = chosen.shape[0]
    per_row = chosen.shape[1]
    flat_ids = chosen.reshape(-1)
    one_hot = (flat_ids[:, None] == jnp.arange(experts_all, dtype=jnp.int32)[None, :]).astype(
        jnp.int32
    )
    within = jnp.sum((jnp.cumsum(one_hot, axis=0) - 1) * one_hot, axis=1)
    slot_index = flat_ids * capacity + within
    row_of = jnp.arange(n_rows * per_row, dtype=jnp.int32) // per_row
    slot_owner = jnp.full((experts_all * capacity,), n_rows, jnp.int32).at[slot_index].set(row_of)
    return (slot_index.reshape(n_rows, per_row), slot_owner)


def mixer_half(queries, key_rows, value_rows, query_gain, key_gain, log_forget, out_weight):
    span_rows = queries.shape[0]
    heads_dev = queries.shape[1] // HEAD_SIZE
    kv_dev = key_rows.shape[1] // HEAD_SIZE
    group_ratio = heads_dev // kv_dev
    scale_qk = HEAD_SIZE ** (-0.5)
    q_normed = head_norm(
        queries.reshape(span_rows, kv_dev, group_ratio, HEAD_SIZE), query_gain
    ).astype(jnp.bfloat16)
    k_normed = head_norm(key_rows.reshape(span_rows, kv_dev, HEAD_SIZE), key_gain).astype(
        jnp.bfloat16
    )
    key_value = jnp.concatenate(
        [k_normed.reshape(span_rows, kv_dev * HEAD_SIZE), value_rows], axis=1
    )
    first_row = lax.axis_index("ep") * span_rows
    last_row = first_row + span_rows - 1
    query_pos = first_row + jnp.arange(span_rows, dtype=jnp.int32)
    query_gates = lax.dynamic_slice_in_dim(log_forget, first_row, span_rows, 1)
    query_gates = query_gates.T.reshape(span_rows, kv_dev, group_ratio)

    def add_block(running, kv_block, key_start):
        run_max, run_sum, run_acc = running
        block_len = kv_block.shape[0]
        k_block = kv_block[:, : kv_dev * HEAD_SIZE].reshape(block_len, kv_dev, HEAD_SIZE)
        v_block = kv_block[:, kv_dev * HEAD_SIZE :].reshape(block_len, kv_dev, HEAD_SIZE)
        key_gates = lax.dynamic_slice_in_dim(log_forget, key_start, block_len, 1)
        key_gates = key_gates.reshape(kv_dev, group_ratio, block_len)
        scores = (
            jnp.einsum("qgrd,kgd->qgrk", q_normed, k_block, preferred_element_type=jnp.float32)
            * scale_qk
        )
        scores = scores + query_gates[..., None] - key_gates[None]
        key_pos = key_start + jnp.arange(block_len, dtype=jnp.int32)
        visible = key_pos[None, :] <= query_pos[:, None]
        scores = jnp.where(visible[:, None, None, :], scores, -jnp.inf)
        new_max = jnp.maximum(run_max, jnp.max(scores, axis=-1))
        shrink = jnp.exp(run_max - new_max)
        weights = jnp.exp(scores - new_max[..., None])
        run_sum = shrink * run_sum + jnp.sum(weights, axis=-1)
        gathered = jnp.einsum(
            "qgrk,kgd->qgrd",
            weights.astype(jnp.bfloat16),
            v_block,
            preferred_element_type=jnp.float32,
        )
        return (new_max, run_sum, shrink[..., None] * run_acc + gathered)

    start_state = (
        jnp.full((span_rows, kv_dev, group_ratio), -jnp.inf, jnp.float32),
        jnp.zeros((span_rows, kv_dev, group_ratio), jnp.float32),
        jnp.zeros((span_rows, kv_dev, group_ratio, HEAD_SIZE), jnp.float32),
    )
    kv_piece = lax.all_gather(key_value, "ep", axis=0, tiled=True)
    block_len = min(kv_piece.shape[0], span_rows)
    n_blocks = kv_piece.shape[0] // block_len

    def one_block(block_number, running_in):
        key_start = block_number * block_len
        kv_block = lax.dynamic_slice_in_dim(kv_piece, block_number * block_len, block_len, 0)

        def take_block(running_now):
            return add_block(running_now, kv_block, key_start)

        def skip_block(running_now):
            return running_now

        return lax.cond(key_start <= last_row, take_block, skip_block, running_in)

    run_max, run_sum, run_acc = lax.fori_loop(0, n_blocks, one_block, start_state)
    attended = (
        (run_acc / run_sum[..., None])
        .astype(jnp.bfloat16)
        .reshape(span_rows, heads_dev * HEAD_SIZE)
    )
    return jnp.dot(attended, out_weight, preferred_element_type=jnp.float32).astype(jnp.bfloat16)


def experts_half(
    expert_rows, expert_gain, routes, route_weight, gate_weight, up_weight, down_weight
):
    n_tp = lax.axis_size("tp")
    n_ep = lax.axis_size("ep")
    span_rows = expert_rows.shape[0]
    model_width = expert_rows.shape[1]
    exp_dev = gate_weight.shape[0]
    capacity = n_tp * ((3 * (span_rows // n_tp) * TOP + 2 * EXPERTS - 1) // (2 * EXPERTS))
    normed = head_norm(expert_rows, expert_gain).astype(jnp.bfloat16)
    slot_index, slot_owner = slot_table(routes.T, EXPERTS, capacity)
    padded = jnp.concatenate([normed, jnp.zeros((1, model_width), jnp.bfloat16)], axis=0)
    part_len = capacity // n_tp
    owner_part = lax.dynamic_slice_in_dim(
        slot_owner.reshape(EXPERTS, capacity), lax.axis_index("tp") * part_len, part_len, 1
    )
    send_rows = padded[owner_part].reshape(n_ep, exp_dev, part_len, model_width)
    arrived = lax.all_to_all(send_rows, "ep", split_axis=0, concat_axis=0, tiled=True)
    slot_rows = lax.all_gather(arrived, "tp", axis=2, tiled=True)
    gate_part = jnp.einsum(
        "nxcd,xdf->nxcf", slot_rows, gate_weight, preferred_element_type=jnp.float32
    )
    up_part = jnp.einsum("nxcd,xdf->nxcf", slot_rows, up_weight, preferred_element_type=jnp.float32)
    hidden = (jax.nn.silu(gate_part) * up_part).astype(jnp.bfloat16)
    partial_out = jnp.einsum(
        "nxcf,xfd->nxcd", hidden, down_weight, preferred_element_type=jnp.float32
    )
    summed = lax.psum_scatter(
        partial_out.astype(jnp.bfloat16), "tp", scatter_dimension=3, tiled=True
    )
    returned = lax.all_to_all(summed, "ep", split_axis=0, concat_axis=0, tiled=True)
    result_table = returned.reshape(EXPERTS * capacity, returned.shape[3])
    picked = result_table[slot_index]
    combined = jnp.sum(picked.astype(jnp.float32) * route_weight.T[..., None], axis=1)
    return combined.astype(jnp.bfloat16)

def route_plan(routes, route_weight, n_dest, exp_dev, row_cap):
    span_rows = routes.shape[1]
    picks = routes[:, :, None] == jnp.arange(EXPERTS, dtype=jnp.int32)
    dest = routes[0] // exp_dev
    to_dest = dest[:, None] == jnp.arange(n_dest, dtype=jnp.int32)
    marks = jnp.concatenate([picks[0] | picks[1], to_dest], axis=1).astype(jnp.bfloat16)
    tokens = jnp.arange(span_rows, dtype=jnp.int32)
    earlier = (tokens[None, :] < tokens[:, None]).astype(jnp.bfloat16)
    ahead = jnp.dot(earlier, marks, preferred_element_type=jnp.float32)
    rank = jnp.sum(jnp.where(to_dest, ahead[:, EXPERTS:], 0.0), axis=1)
    columns = []
    for j in range(TOP):
        within = jnp.sum(jnp.where(picks[j], ahead[:, :EXPERTS], 0.0), axis=1)
        columns += [(routes[j] % exp_dev + 1).astype(jnp.float32), within]
    for j in range(TOP):
        high = lax.reduce_precision(route_weight[j], 8, 7)
        columns += [high, route_weight[j] - high]
    meta = jnp.pad(jnp.stack(columns, axis=1), ((0, 0), (0, META - len(columns))))
    return dest * row_cap + rank.astype(jnp.int32), meta.astype(jnp.bfloat16)


def ring_peers(n_ep, n_tp):
    me = lax.axis_index("ep")
    mine = lax.axis_index("tp")
    pair = mine + 1 - 2 * (mine % 2)
    across = (mine + n_tp // 2) % n_tp
    return me, mine, pair, across


def meet(me, pair, across, n_ep):
    barrier = pltpu.get_barrier_semaphore()
    peers = [{"ep": (me + k) % n_ep} for k in range(1, n_ep)] + [{"tp": pair}, {"tp": across}]
    for peer in peers:
        pl.semaphore_signal(
            barrier, inc=1, device_id=peer, device_id_type=pl.DeviceIdType.MESH
        )
    pl.semaphore_wait(barrier, len(peers))


def remote(src, dst, send_sem, recv_sem, peer):
    return pltpu.make_async_remote_copy(
        src_ref=src,
        dst_ref=dst,
        send_sem=send_sem,
        recv_sem=recv_sem,
        device_id=peer,
        device_id_type=pl.DeviceIdType.MESH,
    )


def spread_kernel(
    n_ep, n_tp, send_ref, out_ref, own_sem, z_send, z_recv, x_send, x_recv, c_send, c_recv
):
    me, mine, pair, across = ring_peers(n_ep, n_tp)
    meet(me, pair, across, n_ep)
    along = []
    for k in range(1, n_ep):
        dest = (me + k) % n_ep
        copy = remote(
            send_ref.at[dest], out_ref.at[me, mine], z_send.at[k], z_recv.at[k], {"ep": dest}
        )
        copy.start()
        along.append(copy)
    own = pltpu.make_async_copy(send_ref.at[me], out_ref.at[me, mine], own_sem)
    own.start()
    crossing = []
    pairing = []

    def pass_on(k):
        source = (me + n_ep - k) % n_ep
        block = send_ref.at[me] if k == 0 else out_ref.at[source, mine]
        place = out_ref.at[source, mine]
        copy = remote(block, place, x_send.at[k], x_recv.at[k], {"tp": across})
        copy.start()
        crossing.append(copy)
        copy = remote(block, place, c_send.at[0, k], c_recv.at[0, k], {"tp": pair})
        copy.start()
        pairing.append(copy)

    def relay(k):
        source = (me + n_ep - k) % n_ep
        crossing[k].wait_recv()
        place = out_ref.at[source, across]
        copy = remote(place, place, c_send.at[1, k], c_recv.at[1, k], {"tp": pair})
        copy.start()
        pairing.append(copy)

    pass_on(0)
    for k in range(1, n_ep):
        along[k - 1].wait_recv()
        pass_on(k)
        relay(k - 1)
    relay(n_ep - 1)
    for copy in pairing:
        copy.wait()
    for copy in crossing + along:
        copy.wait_send()
    own.wait()


def spread_rows(send_rows):
    n_ep = lax.axis_size("ep")
    n_tp = lax.axis_size("tp")
    if n_tp != 4:
        arrived = lax.all_to_all(send_rows, "ep", split_axis=0, concat_axis=0, tiled=True)
        return lax.all_gather(arrived, "tp", axis=1, tiled=True)
    _, part_len, width = send_rows.shape
    dma = pltpu.SemaphoreType.DMA
    arrived = pl.pallas_call(
        functools.partial(spread_kernel, n_ep, n_tp),
        out_shape=jax.ShapeDtypeStruct((n_ep, n_tp, part_len, width), send_rows.dtype),
        in_specs=[pl.BlockSpec(memory_space=pltpu.VMEM)],
        out_specs=pl.BlockSpec(memory_space=pltpu.VMEM),
        scratch_shapes=[
            dma,
            dma((n_ep,)),
            dma((n_ep,)),
            dma((n_ep,)),
            dma((n_ep,)),
            dma((2, n_ep)),
            dma((2, n_ep)),
        ],
        compiler_params=pltpu.CompilerParams(
            collective_id=0, has_side_effects=True, vmem_limit_bytes=16 * 2**20
        ),
        cost_estimate=pl.CostEstimate(flops=0, bytes_accessed=50_000_000, transcendentals=0),
    )(send_rows)
    return arrived.reshape(n_ep, n_tp * part_len, width)


def return_kernel(
    n_ep,
    n_tp,
    rows_ref,
    after_ref,
    out_ref,
    paired,
    leaving,
    crossed,
    final,
    c_send,
    c_recv,
    x_send,
    x_recv,
    z_send,
    z_recv,
):
    me, mine, pair, across = ring_peers(n_ep, n_tp)
    meet(me, pair, across, n_ep)
    width = out_ref.shape[2]
    pair_across = (pair + n_tp // 2) % n_tp

    def columns(quarter):
        return pl.ds(pl.multiple_of(quarter * width, width), width)

    order = list(range(1, n_ep)) + [0]
    pairing = {}
    for k in order:
        dest = (me + k) % n_ep
        for side, quarter in ((1, pair_across), (0, pair)):
            copy = remote(
                rows_ref.at[dest, :, columns(quarter)],
                paired.at[side, k],
                c_send.at[side, k],
                c_recv.at[side, k],
                {"tp": pair},
            )
            copy.start()
            pairing[side, k] = copy
    crossing = {}
    for k in order:
        dest = (me + k) % n_ep
        pairing[1, k].wait_recv()
        both = rows_ref[dest, :, columns(across)].astype(jnp.float32) + paired[1, k].astype(
            jnp.float32
        )
        leaving[k] = both.astype(leaving.dtype)
        copy = remote(leaving.at[k], crossed.at[k], x_send.at[k], x_recv.at[k], {"tp": across})
        copy.start()
        crossing[k] = copy
    along = []
    for k in order:
        dest = (me + k) % n_ep
        pairing[0, k].wait_recv()
        crossing[k].wait_recv()
        total = rows_ref[dest, :, columns(mine)].astype(jnp.float32) + paired[0, k].astype(
            jnp.float32
        )
        total = (total + crossed[k].astype(jnp.float32)).astype(out_ref.dtype)
        if k == 0:
            out_ref[me] = total
        else:
            final[k] = total
            copy = remote(final.at[k], out_ref.at[me], z_send.at[k], z_recv.at[k], {"ep": dest})
            copy.start()
            along.append(copy)
    for copy in along:
        copy.wait()
    for copy in list(pairing.values()) + list(crossing.values()):
        copy.wait_send()


def return_rows(partial_rows, after):
    n_ep = lax.axis_size("ep")
    n_tp = lax.axis_size("tp")
    if n_tp != 4:
        summed = lax.psum_scatter(partial_rows, "tp", scatter_dimension=2, tiled=True)
        return lax.all_to_all(summed, "ep", split_axis=0, concat_axis=0, tiled=True)
    _, row_cap, model_width = partial_rows.shape
    width = model_width // n_tp
    dma = pltpu.SemaphoreType.DMA
    kind = partial_rows.dtype
    return pl.pallas_call(
        functools.partial(return_kernel, n_ep, n_tp),
        out_shape=jax.ShapeDtypeStruct((n_ep, row_cap, width), kind),
        in_specs=[
            pl.BlockSpec(memory_space=pltpu.VMEM),
            pl.BlockSpec(memory_space=pl.ANY),
        ],
        out_specs=pl.BlockSpec(memory_space=pltpu.VMEM),
        scratch_shapes=[
            pltpu.VMEM((2, n_ep, row_cap, width), kind),
            pltpu.VMEM((n_ep, row_cap, width), kind),
            pltpu.VMEM((n_ep, row_cap, width), kind),
            pltpu.VMEM((n_ep, row_cap, width), kind),
            dma((2, n_ep)),
            dma((2, n_ep)),
            dma((n_ep,)),
            dma((n_ep,)),
            dma((n_ep,)),
            dma((n_ep,)),
        ],
        compiler_params=pltpu.CompilerParams(
            collective_id=1, has_side_effects=True, vmem_limit_bytes=20 * 2**20
        ),
        cost_estimate=pl.CostEstimate(flops=0, bytes_accessed=50_000_000, transcendentals=0),
    )(partial_rows, after)


def grouped_experts_half(
    expert_rows,
    expert_gain,
    routes,
    route_weight,
    gate_weight,
    up_weight,
    down_weight,
    mixer_part,
):
    n_tp = lax.axis_size("tp")
    n_ep = lax.axis_size("ep")
    span_rows, model_width = expert_rows.shape
    exp_dev = gate_weight.shape[0]
    capacity = n_tp * ((3 * (span_rows // n_tp) * TOP + 2 * EXPERTS - 1) // (2 * EXPERTS))
    row_cap = exp_dev * capacity // TOP
    part_len = row_cap // n_tp
    row_of, meta = route_plan(routes, route_weight, n_ep, exp_dev, row_cap)
    normed = head_norm(expert_rows, expert_gain).astype(jnp.bfloat16)
    wanted = jnp.arange(n_ep, dtype=jnp.int32)[:, None] * row_cap + (
        lax.axis_index("tp") * part_len + jnp.arange(part_len, dtype=jnp.int32)
    )
    select = (wanted.reshape(-1)[:, None] == row_of[None, :]).astype(jnp.bfloat16)
    send_rows = jnp.dot(
        select, jnp.concatenate([normed, meta], axis=1), preferred_element_type=jnp.float32
    ).astype(jnp.bfloat16)
    arrived = spread_rows(send_rows.reshape(n_ep, part_len, model_width + META))
    arrived, mixer_part = lax.optimization_barrier((arrived, mixer_part))
    notes = arrived[:, :, model_width : model_width + 8].astype(jnp.float32)
    slots = jnp.arange(exp_dev * capacity, dtype=jnp.float32)
    hits = []
    for j in range(TOP):
        local = notes[:, :, 2 * j]
        slot = jnp.where(local > 0, (local - 1) * capacity + notes[:, :, 2 * j + 1], -1.0)
        hits.append(slot[:, :, None] == slots)
    slot_rows = jnp.einsum(
        "nrq,nrd->nqd",
        (hits[0] | hits[1]).astype(jnp.bfloat16),
        arrived[:, :, :model_width],
        preferred_element_type=jnp.float32,
    ).astype(jnp.bfloat16)
    slot_rows = slot_rows.reshape(n_ep, exp_dev, capacity, model_width)
    gate_part = jnp.einsum(
        "nxcd,xdf->nxcf", slot_rows, gate_weight, preferred_element_type=jnp.float32
    )
    up_part = jnp.einsum("nxcd,xdf->nxcf", slot_rows, up_weight, preferred_element_type=jnp.float32)
    hidden = (jax.nn.silu(gate_part) * up_part).astype(jnp.bfloat16)
    down_part = jnp.einsum(
        "nxcf,xfd->nxcd", hidden, down_weight, preferred_element_type=jnp.float32
    ).astype(jnp.bfloat16)
    down_part = down_part.reshape(n_ep, exp_dev * capacity, model_width)
    partial_rows = 0.0
    for piece in range(2):
        weights = sum(
            jnp.where(hits[j], notes[:, :, 2 * TOP + 2 * j + piece][:, :, None], 0.0)
            for j in range(TOP)
        )
        partial_rows = partial_rows + jnp.einsum(
            "nrq,nqd->nrd",
            weights.astype(jnp.bfloat16),
            down_part,
            preferred_element_type=jnp.float32,
        )
    returned = return_rows(partial_rows.astype(jnp.bfloat16), mixer_part[:16, :128])
    returned = returned.reshape(n_ep * row_cap, model_width // n_tp)
    all_rows = jnp.arange(n_ep * row_cap, dtype=jnp.int32)
    return jnp.dot(
        (row_of[:, None] == all_rows[None, :]).astype(jnp.bfloat16),
        returned,
        preferred_element_type=jnp.float32,
    ).astype(jnp.bfloat16)


def on_device(
    queries,
    key_rows,
    value_rows,
    query_gain,
    key_gain,
    log_forget,
    out_weight,
    expert_rows,
    expert_gain,
    routes,
    route_weight,
    gate_weight,
    up_weight,
    down_weight,
):
    mixer_part = mixer_half(
        queries, key_rows, value_rows, query_gain, key_gain, log_forget, out_weight
    )
    expert_args = (
        expert_rows,
        expert_gain,
        routes,
        route_weight,
        gate_weight,
        up_weight,
        down_weight,
    )
    if gate_weight.shape[0] % GROUP_SIZE == 0:
        expert_out = grouped_experts_half(*expert_args, mixer_part)
    else:
        expert_out = experts_half(*expert_args)
    mixer_out = lax.psum_scatter(mixer_part, "tp", scatter_dimension=0, tiled=True)
    return (mixer_out, expert_out)


def solution(mesh):
    in_specs = (
        P(("grp", "ep"), "tp"),
        P(("grp", "ep"), "tp"),
        P(("grp", "ep"), "tp"),
        P(),
        P(),
        P("tp", "grp"),
        P("tp", None),
        P(("grp", "ep"), None),
        P(),
        P(None, ("grp", "ep")),
        P(None, ("grp", "ep")),
        P("ep", None, "tp"),
        P("ep", None, "tp"),
        P("ep", "tp", None),
    )
    out_specs = (P(("grp", "ep", "tp"), None), P(("grp", "ep"), "tp"))
    return jax.shard_map(
        on_device, mesh=mesh, in_specs=in_specs, out_specs=out_specs, check_vma=False
    )
```

profile of v0, /device:TPU:0, one launch (start us, length us, event | category | flops | bytes accessed | tf_op | source)
XLA Modules:
  0.0 161.8 jit_solution(12535462204321179331)
XLA Ops:
  7.2 0.0 all-gather.2.cloned.1.call-start
  7.2 1.1 fusion.73
  8.4 1.0 fusion.75
  9.4 1.6 %pad_maximum_fusion = bf16[512,256]{1,0:T(8,128)(2,1)} fusion(bf16[512,128]{1,0:T(8,128)(2,1)} %param.20, bf16[512,128]{1,0:T(8,128)(2,1)S(1)} %fusion.75), kind=kLoop, calls=%fused_computation.103 | loop fusion | flops 524288 | bytes 524288 | tf_op jit(solution)/shard_map/concatenate | solution.py:49
  11.1 0.0 all-gather.2.cloned.1.call-update
  11.1 0.0 reduce-scatter.2.cloned.1.call-start
  11.2 0.7 slice.73
  11.8 0.8 fusion.91
  12.6 0.7 iota_compare_fusion.9
  13.4 0.2 fusion.49
  13.6 0.1 select_reduce_fusion
  13.8 0.1 broadcast_add_fusion.1
  13.8 0.7 add.247
  14.5 2.1 %fusion.23 = f32[512]{0:T(512)S(1)} fusion(bf16[512,2048]{1,0:T(8,128)(2,1)} %param.25), kind=kLoop, calls=%fused_computation.38 | loop fusion | flops 3145216 | bytes 2099200 | tf_op jit(solution)/shard_map/reduce_sum | solution.py:19
  16.6 0.6 convert_element_type.143
  17.2 0.2 copy.32
  17.4 1.1 copy.21
  18.5 0.1 fusion.65
  18.6 1.5 fusion.67
  20.1 1.1 copy.22
  21.2 0.7 multiply_add_fusion
  21.9 1.2 fusion.25
  23.2 0.7 convolution_convert_fusion.1
  23.9 43.2 %shard_map.149 = bf16[4,4,48,2176]{3,2,1,0:T(8,128)(2,1)S(1)} custom-call(bf16[4,48,2176]{2,1,0:T(8,128)(2,1)S(1)} %bitcast.126), custom_call_target="tpu_custom_call" | custom-call | bytes 50000000 | tf_op jit(solution)/shard_map/pallas_call | solution.py:259
  67.1 1.7 %copy-done.2 = bf16[4,4,48,2176]{3,2,1,0:T(8,128)(2,1)} copy-done((bf16[4,4,48,2176]{3,2,1,0:T(8,128)(2,1)}, bf16[4,4,48,2176]{3,2,1,0:T(8,128)(2,1)S(1)}, u32[]{:S(2)}) %copy-start.2) | copy-done | bytes 3342360
  68.8 0.0 all-gather.2.cloned.1.call-done
  68.8 0.1 broadcast_in_dim.104
  68.9 4.1 %while.18 = (s32[]{:T(128)}, f32[512,1,2]{0,2,1:T(2,128)S(1)}, f32[512,1,2]{0,2,1:T(2,128)S(1)}, f32[512,1,2,128]{0,3,2,1:T(8,128)S(1)}, s32[]{:T(128)}, /*index...) while((s32[]{:T(128)}, f32[512,1,2]{0,2,1:T(2,128)S(1)}, ...), condition=%wide.region_7.8_spmd.clone, body=%wide.region_2.7_spmd.clone.sunk | while | flops 273682432 | bytes 8483165 | solution.py:106
  68.9 3.7 %conditional.3 = ((f32[512,1,2]{0,2,1:T(2,128)S(1)}, f32[512,1,2]{0,2,1:T(2,128)S(1)}, f32[512,1,2,128]{0,3,2,1:T(8,128)S(1)})) conditional(s32[]{:T(128)} %convert_element_type.207, (f32[512,1,2]{0,2,1:T(2,128)S(1)}, f32[512,1,2]{0,2,1:T(2,128)S(1)}, f32[512,1,2,128]{0,3,2,1:T(8,128)S(1)}) %tuple.68, (s32[]{:T(128)}, s32[]{:T(128)}, ...), branch_computations={%region_3.0_spmd, %region_4.6_spmd} | conditional | flops 273682432 | bytes 8480870 | solution.py:104
  69.0 0.2 broadcast_compare_fusion
  69.2 1.6 fusion.102
  70.8 1.5 fusion.5
  72.3 0.3 fusion.4
  73.0 0.1 divide_convert_fusion
  73.1 2.1 %convolution_convert_fusion.2 = bf16[512,2048]{1,0:T(8,128)(2,1)} fusion(bf16[512,256]{0,1:T(8,128)(2,1)S(1)} %bitcast.135, bf16[256,2048]{1,0:T(8,128)(2,1)S(1)} %copy-done), kind=kOutput, calls=%fused_computation.43 | convolution fusion | flops 537919488 | bytes 3407872 | tf_op jit(solution)/shard_map/dot_general | solution.py:112
  75.2 0.0 reduce-scatter.2.cloned.1.call-update
  75.2 1.1 slice_convert_fusion
  76.3 1.6 %slice_reduce_fusion.1 = (f32[4,192]{1,0:T(4,128)S(1)}, f32[4,192]{1,0:T(4,128)S(1)}, f32[4,192]{1,0:T(4,128)S(1)}, f32[4,192]{1,0:T(4,128)S(1)}, f32[4,192]{1,0:T(4,128)S(1)}, /*index=5*/f32[4,192]{1,0:T(4,128)S(1)}) fusion(f32[4,192,8]{2,1,0:T(8,128)S(1)} %slice_convert_fusion), kind=kLoop, calls=%fused_computation.88 | loop fusion | flops 7680 | bytes 43008 | tf_op jit(solution)/shard_map/slice | solution.py:444
  78.0 1.9 %convolution_convert_fusion = bf16[4,384,2048]{2,1,0:T(8,128)(2,1)S(1)} fusion(bf16[4,192,2176]{2,1,0:T(8,128)(2,1)S(1)} %bitcast.125, f32[4,192]{1,0:T(4,128)S(1)} %get-tuple-element.319, f32[4,192]{1,0:T(4,128)S(1)} %get-tuple-element.322), kind=kOutput, calls=%fused_computation.35 | convolution fusion | flops 1211990016 | bytes 9445376 | tf_op jit(solution)/shard_map/nrq,nrd->nqd/dot_general | solution.py:425
  79.9 0.7 slice.91.after_ref
  80.6 2.0 %copy-done.5 = bf16[4,384,2048]{2,1,0:T(8,128)(2,1)} copy-done((bf16[4,384,2048]{2,1,0:T(8,128)(2,1)}, bf16[4,384,2048]{2,1,0:T(8,128)(2,1)S(1)}, u32[]{:S(2)}) %copy-start.5) | copy-done | bytes 6291480
  82.6 5.3 %fusion.16 = f32[8,4,48,256]{3,2,1,0:T(8,128)S(1)} fusion(bf16[8,2048,256]{2,1,0:T(8,128)(2,1)} %param.29, bf16[4,8,48,2048]{3,2,1,0:T(8,128)(2,1)S(1)} %bitcast.130), kind=kOutput, calls=%fused_computation.27 | convolution fusion | flops 1610612736 | bytes 16252928 | tf_op jit(solution)/shard_map/nxcd,xdf->nxcf/dot_general | solution.py:432
  87.9 13.9 %convert_bitcast_fusion = bf16[4,8,48,2048]{3,2,0,1:T(8,128)(2,1)} fusion(bf16[8,256,2048]{2,1,0:T(8,128)(2,1)} %param.31, f32[8,4,48,256]{3,2,1,0:T(8,128)S(1)} %fusion.16, bf16[8,2048,256]{2,1,0:T(8,128)(2,1)} %param.30, bf16[4,8,48,2048]{3,2,1,0:T(8,128)(2,1)} %bitcast.131), kind=kOutput, calls=%fused_computation.30 | convolution fusion | flops 3226730496 | bytes 30932992 | tf_op jit(solution)/shard_map/nxcf,xfd->nxcd/dot_general | solution.py:437
  101.8 3.4 %copy.25 = bf16[4,8,48,2048]{3,2,1,0:T(8,128)(2,1)S(1)} copy(bf16[4,8,48,2048]{3,2,0,1:T(8,128)(2,1)} %convert_bitcast_fusion) | data formatting | bytes 12582912 | tf_op jit(solution)/shard_map/convert_element_type | solution.py:439
  105.1 1.9 %fusion.52 = f32[4,192,2048]{2,1,0:T(8,128)S(1)} fusion(bf16[4,384,2048]{2,1,0:T(8,128)(2,1)S(1)} %bitcast.128, f32[4,192]{1,0:T(4,128)S(1)} %get-tuple-element.318, f32[4,192]{1,0:T(4,128)S(1)} %get-tuple-element.319, f32[4,192]{1,0:T(4,128)S(1)} %get-tuple-element.321, f32[4,192]{1,0:T(4,128)S(1)} %get-tuple-element.322), kind=kOutput, calls=%fused_computation.70 | convolution fusion | flops 1209729024 | bytes 12595200 | tf_op jit(solution)/shard_map/nrq,nqd->nrd/dot_general | solution.py:447
  107.1 2.2 %add_convert_fusion.rows_ref = bf16[4,192,2048]{2,1,0:T(8,128)(2,1)S(1)} fusion(f32[4,192,2048]{2,1,0:T(8,128)S(1)} %fusion.52, bf16[4,384,2048]{2,1,0:T(8,128)(2,1)S(1)} %bitcast.129, f32[4,192]{1,0:T(4,128)S(1)} %get-tuple-element.320, f32[4,192]{1,0:T(4,128)S(1)} %get-tuple-element.317, f32[4,192]{1,0:T(4,128)S(1)} %get-tuple-element.319, ...), kind=kOutput, calls=%fused_computation.29 | convolution fusion | flops 1212874752 | bytes 15740928 | tf_op jit(solution)/shard_map/nrq,nqd->nrd/dot_general | solution.py:447
  109.3 44.2 %shard_map.150 = bf16[4,192,512]{2,1,0:T(8,128)(2,1)S(1)} custom-call(bf16[4,192,2048]{2,1,0:T(8,128)(2,1)S(1)} %add_convert_fusion.rows_ref, bf16[16,128]{1,0:T(8,128)(2,1)S(1)} %slice.91.after_ref), custom_call_target="tpu_custom_call" | custom-call | bytes 50000000 | tf_op jit(solution)/shard_map/pallas_call | solution.py:363
  153.6 1.4 fusion.45
  (48 shorter events, 0.3 us)
Async XLA Ops:
  7.2 65.9 %copy-start = (bf16[256,2048]{1,0:T(8,128)(2,1)S(1)}, bf16[256,2048]{1,0:T(8,128)(2,1)}, u32[]{:S(2)}) copy-start(bf16[256,2048]{1,0:T(8,128)(2,1)} %param.24) | copy-start | bytes 3145732
  7.2 9.4 %copy-start.8 = (f32[2,512]{1,0:T(2,128)S(1)}, f32[2,512]{1,0:T(2,128)}, u32[]{:S(2)}) copy-start(f32[2,512]{1,0:T(2,128)} %param.28) | copy-start | bytes 12292
  7.2 61.6 %all-gather.2.cloned.1.call-start = ((), (), s32[]{:S(2)}) async-start(), calls=%async_computation.1 | async-start | bytes 1310720 | tf_op jit(solution)/shard_map/all_gather | solution.py:90
  11.1 143.9 %reduce-scatter.2.cloned.1.call-start = ((), (), s32[]{:S(2)}) async-start(), calls=%async_computation.2 | async-start | bytes 2621440 | tf_op jit(solution)/shard_map/reduce_scatter | solution.py:495
  13.7 7.5 %copy-start.7 = (s32[2,512]{1,0:T(2,128)S(1)}, s32[2,512]{1,0:T(2,128)}, u32[]{:S(2)}) copy-start(s32[2,512]{1,0:T(2,128)} %param.27) | copy-start | bytes 12292
  13.7 8.2 %copy-start.4 = (bf16[512,2048]{1,0:T(8,128)(2,1)S(1)}, bf16[512,2048]{1,0:T(8,128)(2,1)}, u32[]{:S(2)}) copy-start(bf16[512,2048]{1,0:T(8,128)(2,1)} %param.25) | copy-start | bytes 6291460
  21.9 1.3 copy-start.9
  23.9 44.9 %copy-start.6 = (f32[2,2048]{1,0:T(2,128)S(1)}, f32[2,2048]{1,0:T(2,128)}, u32[]{:S(2)}) copy-start(f32[2,2048]{1,0:T(2,128)} %param.23) | copy-start | bytes 49156
  67.1 1.7 %copy-start.2 = (bf16[4,4,48,2176]{3,2,1,0:T(8,128)(2,1)}, bf16[4,4,48,2176]{3,2,1,0:T(8,128)(2,1)S(1)}, u32[]{:S(2)}) copy-start(bf16[4,4,48,2176]{3,2,1,0:T(8,128)(2,1)S(1)} %shard_map.149) | copy-start | bytes 10027012
  75.2 2.8 %copy-start.3 = (bf16[4,4,48,2176]{3,2,1,0:T(8,128)(2,1)S(1)}, bf16[4,4,48,2176]{3,2,1,0:T(8,128)(2,1)}, u32[]{:S(2)}) copy-start(bf16[4,4,48,2176]{3,2,1,0:T(8,128)(2,1)} %copy-done.2) | copy-start | bytes 10027012
  79.9 2.7 %copy-start.5 = (bf16[4,384,2048]{2,1,0:T(8,128)(2,1)}, bf16[4,384,2048]{2,1,0:T(8,128)(2,1)S(1)}, u32[]{:S(2)}) copy-start(bf16[4,384,2048]{2,1,0:T(8,128)(2,1)S(1)} %convolution_convert_fusion) | copy-start | bytes 18874372
  109.3 45.7 %copy-start.1 = (bf16[256,2048]{1,0:T(8,128)(2,1)S(1)}, bf16[256,2048]{1,0:T(8,128)(2,1)}, u32[]{:S(2)}) copy-start(bf16[256,2048]{1,0:T(8,128)(2,1)} %param.24) | copy-start | bytes 3145732
Sparse Core Ops, SparseCore 0:
  11.2 45.9 all-gather.1
  75.3 45.8 reduce-scatter.1
where the time goes:
time: 162 us
  Pallas kernels  87.4 us (54%)
  matrix products  32.8 us (20%)
  other arithmetic  15 us (9%)
  between operations  14.4 us (9%)
  local copies, waits for them, and re-layouts  11.6 us (7%)
    pallas_call x1, Pallas kernels, return_rows(): pl.pallas_call(functools.partial(return_kernel, n_ep, n_tp), out_shape=ja...  44.2 us
    pallas_call x1, Pallas kernels, spread_rows(): pl.pallas_call(functools.partial(spread_kernel, n_ep, n_tp), out_shape=ja...  43.2 us
    dot_general x1, matrix products, grouped_experts_half(): jnp.einsum('nxcf,xfd->nxcd', hidden, down_weight, preferred_element_type=...  13.9 us
    unnamed x23, local copies, waits for them, and re-layouts  6.09 us
    dot_general x1, matrix products, grouped_experts_half(): jnp.einsum('nxcd,xdf->nxcf', slot_rows, gate_weight, preferred_element_ty...  5.26 us
    dot_general x2, matrix products, grouped_experts_half(): jnp.einsum('nrq,nqd->nrd', weights.astype(jnp.bfloat16), down_part, prefe...  4.14 us
    convert_element_type x1, local copies, waits for them, and re-layouts, grouped_experts_half(): down_part = jnp.einsum('nxcf,xfd->nxcd', hidden, down_weight, preferred_e...  3.36 us
    reduce_sum x3, other arithmetic, head_norm(): jnp.mean(widened * widened, axis=-1, keepdims=True) + 1e-06  3.27 us
  transfers between devices with their start and end apart: 2, of which 0 were waited for; matrix products, arithmetic and copies ran while one was open for 28% of the time, Pallas kernels for 54%

commit v1 on v0

v1 whole, which is shorter than its diff:
```python
import functools

import jax
import jax.numpy as jnp
from jax import lax
from jax.experimental import pallas as pl
from jax.experimental.pallas import tpu as pltpu
from jax.sharding import PartitionSpec as P

HEAD_SIZE = 128
EXPERTS = 32
TOP = 2
GROUP_SIZE = 8
VMEM_LIMIT = 65000 * 1024


def head_norm(inputs, scale_gain):
    widened = inputs.astype(jnp.float32)
    factor = lax.rsqrt(jnp.mean(widened * widened, axis=-1, keepdims=True) + 1e-06)
    return widened * factor * scale_gain


def slot_table(chosen, experts_all, capacity):
    n_rows = chosen.shape[0]
    per_row = chosen.shape[1]
    flat_ids = chosen.reshape(-1)
    one_hot = (flat_ids[:, None] == jnp.arange(experts_all, dtype=jnp.int32)[None, :]).astype(
        jnp.int32
    )
    within = jnp.sum((jnp.cumsum(one_hot, axis=0) - 1) * one_hot, axis=1)
    slot_index = flat_ids * capacity + within
    row_of = jnp.arange(n_rows * per_row, dtype=jnp.int32) // per_row
    slot_owner = jnp.full((experts_all * capacity,), n_rows, jnp.int32).at[slot_index].set(row_of)
    return (slot_index.reshape(n_rows, per_row), slot_owner)


def mixer_half(queries, key_rows, value_rows, query_gain, key_gain, log_forget, out_weight):
    span_rows = queries.shape[0]
    heads_dev = queries.shape[1] // HEAD_SIZE
    kv_dev = key_rows.shape[1] // HEAD_SIZE
    group_ratio = heads_dev // kv_dev
    scale_qk = HEAD_SIZE ** (-0.5)
    q_normed = head_norm(
        queries.reshape(span_rows, kv_dev, group_ratio, HEAD_SIZE), query_gain
    ).astype(jnp.bfloat16)
    k_normed = head_norm(key_rows.reshape(span_rows, kv_dev, HEAD_SIZE), key_gain).astype(
        jnp.bfloat16
    )
    key_value = jnp.concatenate(
        [k_normed.reshape(span_rows, kv_dev * HEAD_SIZE), value_rows], axis=1
    )
    first_row = lax.axis_index("ep") * span_rows
    last_row = first_row + span_rows - 1
    query_pos = first_row + jnp.arange(span_rows, dtype=jnp.int32)
    query_gates = lax.dynamic_slice_in_dim(log_forget, first_row, span_rows, 1)
    query_gates = query_gates.T.reshape(span_rows, kv_dev, group_ratio)

    def add_block(running, kv_block, key_start):
        run_max, run_sum, run_acc = running
        block_len = kv_block.shape[0]
        k_block = kv_block[:, : kv_dev * HEAD_SIZE].reshape(block_len, kv_dev, HEAD_SIZE)
        v_block = kv_block[:, kv_dev * HEAD_SIZE :].reshape(block_len, kv_dev, HEAD_SIZE)
        key_gates = lax.dynamic_slice_in_dim(log_forget, key_start, block_len, 1)
        key_gates = key_gates.reshape(kv_dev, group_ratio, block_len)
        scores = (
            jnp.einsum("qgrd,kgd->qgrk", q_normed, k_block, preferred_element_type=jnp.float32)
            * scale_qk
        )
        scores = scores + query_gates[..., None] - key_gates[None]
        key_pos = key_start + jnp.arange(block_len, dtype=jnp.int32)
        visible = key_pos[None, :] <= query_pos[:, None]
        scores = jnp.where(visible[:, None, None, :], scores, -jnp.inf)
        new_max = jnp.maximum(run_max, jnp.max(scores, axis=-1))
        shrink = jnp.exp(run_max - new_max)
        weights = jnp.exp(scores - new_max[..., None])
        run_sum = shrink * run_sum + jnp.sum(weights, axis=-1)
        gathered = jnp.einsum(
            "qgrk,kgd->qgrd",
            weights.astype(jnp.bfloat16),
            v_block,
            preferred_element_type=jnp.float32,
        )
        return (new_max, run_sum, shrink[..., None] * run_acc + gathered)

    start_state = (
        jnp.full((span_rows, kv_dev, group_ratio), -jnp.inf, jnp.float32),
        jnp.zeros((span_rows, kv_dev, group_ratio), jnp.float32),
        jnp.zeros((span_rows, kv_dev, group_ratio, HEAD_SIZE), jnp.float32),
    )
    kv_piece = lax.all_gather(key_value, "ep", axis=0, tiled=True)
    block_len = min(kv_piece.shape[0], span_rows)
    n_blocks = kv_piece.shape[0] // block_len

    def one_block(block_number, running_in):
        key_start = block_number * block_len
        kv_block = lax.dynamic_slice_in_dim(kv_piece, block_number * block_len, block_len, 0)

        def take_block(running_now):
            return add_block(running_now, kv_block, key_start)

        def skip_block(running_now):
            return running_now

        return lax.cond(key_start <= last_row, take_block, skip_block, running_in)

    run_max, run_sum, run_acc = lax.fori_loop(0, n_blocks, one_block, start_state)
    attended = (
        (run_acc / run_sum[..., None])
        .astype(jnp.bfloat16)
        .reshape(span_rows, heads_dev * HEAD_SIZE)
    )
    return jnp.dot(attended, out_weight, preferred_element_type=jnp.float32).astype(jnp.bfloat16)


def experts_half(
    expert_rows, expert_gain, routes, route_weight, gate_weight, up_weight, down_weight
):
    n_tp = lax.axis_size("tp")
    n_ep = lax.axis_size("ep")
    span_rows = expert_rows.shape[0]
    model_width = expert_rows.shape[1]
    exp_dev = gate_weight.shape[0]
    capacity = n_tp * ((3 * (span_rows // n_tp) * TOP + 2 * EXPERTS - 1) // (2 * EXPERTS))
    normed = head_norm(expert_rows, expert_gain).astype(jnp.bfloat16)
    slot_index, slot_owner = slot_table(routes.T, EXPERTS, capacity)
    padded = jnp.concatenate([normed, jnp.zeros((1, model_width), jnp.bfloat16)], axis=0)
    part_len = capacity // n_tp
    owner_part = lax.dynamic_slice_in_dim(
        slot_owner.reshape(EXPERTS, capacity), lax.axis_index("tp") * part_len, part_len, 1
    )
    send_rows = padded[owner_part].reshape(n_ep, exp_dev, part_len, model_width)
    arrived = lax.all_to_all(send_rows, "ep", split_axis=0, concat_axis=0, tiled=True)
    slot_rows = lax.all_gather(arrived, "tp", axis=2, tiled=True)
    gate_part = jnp.einsum(
        "nxcd,xdf->nxcf", slot_rows, gate_weight, preferred_element_type=jnp.float32
    )
    up_part = jnp.einsum("nxcd,xdf->nxcf", slot_rows, up_weight, preferred_element_type=jnp.float32)
    hidden = (jax.nn.silu(gate_part) * up_part).astype(jnp.bfloat16)
    partial_out = jnp.einsum(
        "nxcf,xfd->nxcd", hidden, down_weight, preferred_element_type=jnp.float32
    )
    summed = lax.psum_scatter(
        partial_out.astype(jnp.bfloat16), "tp", scatter_dimension=3, tiled=True
    )
    returned = lax.all_to_all(summed, "ep", split_axis=0, concat_axis=0, tiled=True)
    result_table = returned.reshape(EXPERTS * capacity, returned.shape[3])
    picked = result_table[slot_index]
    combined = jnp.sum(picked.astype(jnp.float32) * route_weight.T[..., None], axis=1)
    return combined.astype(jnp.bfloat16)


LOG2E = 1.4426950408889634


def remote(src, dst, send_sem, recv_sem, peer):
    return pltpu.make_async_remote_copy(
        src_ref=src,
        dst_ref=dst,
        send_sem=send_sem,
        recv_sem=recv_sem,
        device_id=peer,
        device_id_type=pl.DeviceIdType.MESH,
    )


def dot_nt(lhs, rhs):
    return lax.dot_general(
        lhs, rhs, (((1,), (1,)), ((), ())), preferred_element_type=jnp.float32
    )


def dot_nn(lhs, rhs):
    return jnp.dot(lhs, rhs, preferred_element_type=jnp.float32)


def rows_of(index, size):
    return pl.ds(pl.multiple_of(index * size, size), size)


def one_hot(condition):
    return jnp.where(condition, 1.0, 0.0).astype(jnp.bfloat16)


def iota_f32(shape, dim):
    return lax.broadcasted_iota(jnp.int32, shape, dim).astype(jnp.float32)


def fused_kernel(
    n_ep,
    n_tp,
    capacity,
    q_hbm,
    k_hbm,
    v_hbm,
    qg_hbm,
    kg_hbm,
    lf_hbm,
    wo_hbm,
    x_hbm,
    xg_hbm,
    info_hbm,
    wg_hbm,
    wu_hbm,
    wd_hbm,
    mix_ref,
    exp_ref,
    q_in,
    k_in,
    kv,
    qg,
    kg,
    lf,
    wo,
    x_in,
    xg,
    info,
    wg,
    wu,
    wd,
    q_norm,
    run_max,
    run_sum,
    run_acc,
    att,
    mixp,
    mpaired,
    mleaving,
    mcrossed,
    normed,
    earlier,
    send_rows,
    arrived,
    gather_hot,
    return_hot,
    slot_weight,
    final_hot,
    slots,
    down,
    partial,
    paired,
    leaving,
    crossed,
    final,
    returned,
    in_sem,
    w_sem,
    kv_send,
    kv_recv,
    i_send,
    i_recv,
    z_send,
    z_recv,
    x_send,
    x_recv,
    c_send,
    c_recv,
    rc_send,
    rc_recv,
    rx_send,
    rx_recv,
    rz_send,
    rz_recv,
    m_send,
    m_recv,
):
    me = lax.axis_index("ep")
    mine = lax.axis_index("tp")
    pair = mine + 1 - 2 * (mine % 2)
    across = (mine + n_tp // 2) % n_tp
    pair_across = (pair + n_tp // 2) % n_tp
    span, width = x_in.shape
    heads = q_norm.shape[0]
    head = q_norm.shape[2]
    exp_dev = wg.shape[0]
    part = send_rows.shape[1]
    row_cap = part * n_tp
    n_slots = exp_dev * capacity
    quarter = width // n_tp
    score_scale = (head**-0.5) * LOG2E

    fetches = []

    def fetch(src, dst):
        copy = pltpu.make_async_copy(src, dst, in_sem.at[len(fetches)])
        copy.start()
        fetches.append(copy)
        return copy

    get_k = fetch(k_hbm, k_in)
    get_kg = fetch(kg_hbm, kg)
    get_v = fetch(v_hbm, kv.at[0, 1])
    get_info = fetch(info_hbm, info.at[0])
    get_x = fetch(x_hbm, x_in)
    get_xg = fetch(xg_hbm, xg)
    get_q = fetch(q_hbm, q_in)
    get_qg = fetch(qg_hbm, qg)
    get_lf = fetch(lf_hbm, lf)
    get_wo = fetch(wo_hbm, wo)
    weights = []
    for e in range(exp_dev):
        for i, (src, dst) in enumerate(((wg_hbm, wg), (wu_hbm, wu), (wd_hbm, wd))):
            copy = pltpu.make_async_copy(src.at[e], dst.at[e], w_sem.at[i, e])
            copy.start()
            weights.append(copy)

    barrier = pltpu.get_barrier_semaphore()
    peers = [{"ep": (me + k) % n_ep} for k in range(1, n_ep)] + [{"tp": pair}, {"tp": across}]
    for peer in peers:
        pl.semaphore_signal(barrier, inc=1, device_id=peer, device_id_type=pl.DeviceIdType.MESH)

    get_k.wait()
    get_kg.wait()

    def norm_heads(rows, gain):
        factor = lax.rsqrt(jnp.mean(rows * rows, axis=-1, keepdims=True) + 1e-06)
        return (rows * factor * gain).astype(jnp.bfloat16)

    kv[0, 0] = norm_heads(k_in[...].astype(jnp.float32), kg[...])
    get_info.wait()
    get_v.wait()
    pl.semaphore_wait(barrier, len(peers))

    notes_sent = []
    for k in range(1, n_ep):
        copy = remote(
            info_hbm, info.at[k], i_send.at[k], i_recv.at[k], {"ep": (me + k) % n_ep}
        )
        copy.start()
        notes_sent.append(copy)

    kv_copies = [
        remote(kv.at[d], kv.at[d + 1], kv_send.at[d], kv_recv.at[d + 1], {"ep": (me + 1) % n_ep})
        for d in range(n_ep - 1)
    ]

    def kv_pass(d):
        @pl.when((me >= d) & (me < n_ep - 1))
        def _():
            kv_copies[d].start()

    kv_pass(0)

    me_f = me.astype(jnp.float32)
    earlier[...] = one_hot(iota_f32((span, span), 0) < iota_f32((span, span), 1))
    kinds = iota_f32((8, span), 0)

    def ranks(k):
        table = info[k]
        dest = table[0:1]
        at_me = dest == me_f
        local = [jnp.where(at_me, table[1 + j : 2 + j], -1.0) for j in range(TOP)]
        to_dest = jnp.where(dest == kinds, 1.0, 0.0)
        picks = [jnp.where(local[j] == kinds, 1.0, 0.0) for j in range(TOP)]
        marks = jnp.concatenate([to_dest, picks[0] + picks[1]], axis=0).astype(jnp.bfloat16)
        ahead = dot_nn(marks, earlier[...])
        rank = jnp.sum(to_dest * ahead[:8], axis=0, keepdims=True)
        within = [jnp.sum(picks[j] * ahead[8:], axis=0, keepdims=True) for j in range(TOP)]
        return table, dest, at_me, local, rank, within

    def slot_tables(k, ranked):
        table, dest, at_me, local, rank, within = ranked
        row_key = jnp.where(at_me, rank, -1.0)
        picked = one_hot(iota_f32((row_cap, span), 0) == row_key)
        columns = jnp.zeros((8, span), jnp.float32)
        entries = [local[0] + 1.0, within[0], local[1] + 1.0, within[1]]
        entries += [table[3 + i : 4 + i] for i in range(4)]
        for i, entry in enumerate(entries):
            columns = jnp.where(kinds == float(i), entry, columns)
        columns = jnp.concatenate([columns, jnp.zeros((8, span), jnp.float32)], axis=0)
        columns = columns.astype(jnp.bfloat16)
        across_rows = dot_nt(columns, picked)
        along_rows = dot_nt(picked, columns)
        slot_ids = iota_f32((n_slots, row_cap), 0)
        slot_lanes = iota_f32((row_cap, n_slots), 1)
        lane_hits = []
        gains = 0.0
        hot = 0.0
        for j in range(TOP):
            level = across_rows[2 * j : 2 * j + 1]
            slot = jnp.where(
                level > 0.5, (level - 1.0) * capacity + across_rows[2 * j + 1 : 2 * j + 2], -1.0
            )
            weight = across_rows[4 + 2 * j : 5 + 2 * j] + across_rows[5 + 2 * j : 6 + 2 * j]
            match = slot_ids == slot
            hot = hot + jnp.where(match, 1.0, 0.0)
            gains = gains + jnp.where(match, weight, 0.0)
            level = along_rows[:, 2 * j : 2 * j + 1]
            slot = jnp.where(
                level > 0.5, (level - 1.0) * capacity + along_rows[:, 2 * j + 1 : 2 * j + 2], -1.0
            )
            lane_hits.append(jnp.where(slot_lanes == slot, 1.0, 0.0))
        gather_hot[k] = hot.astype(jnp.bfloat16)
        return_hot[k] = (lane_hits[0] + lane_hits[1]).astype(jnp.bfloat16)
        slot_weight[k] = jnp.sum(gains, axis=1, keepdims=True)

    get_x.wait()
    get_xg.wait()
    norm_rows = 32

    def norm_tile(i, carry):
        rows = rows_of(i, norm_rows)
        normed[rows, :] = norm_heads(x_in[rows, :].astype(jnp.float32), xg[...])
        return carry

    lax.fori_loop(0, span // norm_rows, norm_tile, 0)
    own = ranks(0)
    _, dest, _, _, rank, _ = own
    token_key = dest * row_cap + rank
    part_base = (mine * part).astype(jnp.float32)
    part_rows = iota_f32((part, span), 0) + part_base
    chosen = []
    for k in range(1, n_ep):
        base = ((me + k) % n_ep * row_cap).astype(jnp.float32)
        chosen.append(jnp.where(part_rows + base == token_key, 1.0, 0.0))
    chosen = jnp.concatenate(chosen, axis=0).astype(jnp.bfloat16)
    col = 256

    def send_tile(i, carry):
        cols = rows_of(i, col)
        rows = dot_nn(chosen, normed[:, cols]).astype(jnp.bfloat16)
        for k in range(1, n_ep):
            send_rows[k - 1, :, cols] = rows[(k - 1) * part : k * part]
        return carry

    lax.fori_loop(0, width // col, send_tile, 0)
    along = {}
    for k in range(1, n_ep):
        copy = remote(
            send_rows.at[k - 1],
            arrived.at[k, mine],
            z_send.at[k],
            z_recv.at[k],
            {"ep": (me + k) % n_ep},
        )
        copy.start()
        along[k] = copy

    own_rows = one_hot(
        iota_f32((row_cap, span), 0) + (me * row_cap).astype(jnp.float32) == token_key
    )

    def own_tile(i, carry):
        cols = rows_of(i, col)
        rows = dot_nn(own_rows, normed[:, cols]).astype(jnp.bfloat16)
        for p in range(n_tp):
            arrived[0, p, :, cols] = rows[p * part : (p + 1) * part]
        return carry

    lax.fori_loop(0, width // col, own_tile, 0)

    get_q.wait()
    get_qg.wait()
    get_lf.wait()
    for h in range(heads):
        q_norm[h] = norm_heads(
            q_in[:, h * head : (h + 1) * head].astype(jnp.float32), qg[...]
        )
    tile = 256
    first_token = pl.multiple_of(me * span, span)

    def attend(d):
        key_start = pl.multiple_of((me - d) * span, span)
        for h in range(heads):
            start_gate = lf[h : h + 1, pl.ds(first_token, head)][:, 0:1]
            gate = (start_gate - lf[h : h + 1, pl.ds(key_start, span)]) * LOG2E

            def query_tile(i, carry):
                rows = rows_of(i, tile)
                scores = dot_nt(q_norm[h, rows, :], kv[d, 0]) * score_scale + gate
                if d == 0:
                    key_at = lax.broadcasted_iota(jnp.int32, (tile, span), 1)
                    query_at = lax.broadcasted_iota(jnp.int32, (tile, span), 0) + i * tile
                    scores = jnp.where(key_at <= query_at, scores, -jnp.inf)
                top = jnp.max(scores, axis=-1, keepdims=True)
                if d == 0:
                    prob = jnp.exp2(scores - top)
                    run_max[h, rows, :] = top
                    run_sum[h, rows, :] = jnp.sum(prob, axis=-1, keepdims=True)
                    run_acc[h, rows, :] = dot_nn(prob.astype(jnp.bfloat16), kv[d, 1])
                else:
                    old = run_max[h, rows, :]
                    top = jnp.maximum(old, top)
                    shrink = jnp.exp2(old - top)
                    prob = jnp.exp2(scores - top)
                    run_max[h, rows, :] = top
                    run_sum[h, rows, :] = run_sum[h, rows, :] * shrink + jnp.sum(
                        prob, axis=-1, keepdims=True
                    )
                    run_acc[h, rows, :] = run_acc[h, rows, :] * shrink + dot_nn(
                        prob.astype(jnp.bfloat16), kv[d, 1]
                    )
                return carry

            lax.fori_loop(0, span // tile, query_tile, 0)

    attend(0)

    def kv_step(d):
        @pl.when(me >= d)
        def _():
            kv_copies[d - 1].wait_recv()

        if d < n_ep - 1:
            kv_pass(d)

        @pl.when(me >= d)
        def _():
            attend(d)

    crossing = {}
    pairing = {}

    def pass_on(k):
        along[k].wait_recv()
        place = arrived.at[k, mine]
        copy = remote(place, place, x_send.at[k], x_recv.at[k], {"tp": across})
        copy.start()
        crossing[k] = copy
        copy = remote(place, place, c_send.at[0, k], c_recv.at[0, k], {"tp": pair})
        copy.start()
        pairing[0, k] = copy

    def relay(k):
        crossing[k].wait_recv()
        place = arrived.at[k, across]
        copy = remote(place, place, c_send.at[1, k], c_recv.at[1, k], {"tp": pair})
        copy.start()
        pairing[1, k] = copy

    def fill_slots(k, side):
        if k > 0:
            pairing[0, k].wait_recv()
            pairing[1, k].wait_recv()

        def slot_tile(i, carry):
            cols = rows_of(i, col)
            rows = arrived[k, :, :, cols].reshape(row_cap, col)
            filled = dot_nn(gather_hot[k], rows).astype(jnp.bfloat16)
            for e in range(exp_dev):
                slots[e, side * capacity : (side + 1) * capacity, cols] = filled[
                    e * capacity : (e + 1) * capacity
                ]
            return carry

        lax.fori_loop(0, width // col, slot_tile, 0)

    wide = 512

    def expert_pass(sources):
        def one_expert(e, carry):
            rows = slots[e]
            gate_part = dot_nn(rows, wg[e])
            up_part = dot_nn(rows, wu[e])
            weight = jnp.concatenate(
                [slot_weight[k, rows_of(e, capacity), :] for k in sources], axis=0
            )
            hidden = gate_part / (1.0 + jnp.exp(-gate_part)) * up_part * weight
            hidden = hidden.astype(jnp.bfloat16)
            for c in range(width // wide):
                cols = slice(c * wide, (c + 1) * wide)
                result = dot_nn(hidden, wd[e, :, cols]).astype(jnp.bfloat16)
                for side in range(len(sources)):
                    down[side, e, :, cols] = result[side * capacity : (side + 1) * capacity]
            return carry

        lax.fori_loop(0, exp_dev, one_expert, 0)

    back_pairing = {}
    back_crossing = {}
    back_along = {}
    order = list(range(1, n_ep)) + [0]

    def combine(k, side):
        def combine_tile(c, carry):
            cols = rows_of(c, quarter)
            rows = down[side, :, :, cols].reshape(n_slots, quarter)
            partial[k, c] = dot_nn(return_hot[k], rows).astype(jnp.bfloat16)
            return carry

        lax.fori_loop(0, n_tp, combine_tile, 0)
        for way, block in ((1, pair_across), (0, pair)):
            copy = remote(
                partial.at[k, block],
                paired.at[way, k],
                rc_send.at[way, k],
                rc_recv.at[way, k],
                {"tp": pair},
            )
            copy.start()
            back_pairing[way, k] = copy

    def back_cross(k):
        back_pairing[1, k].wait_recv()
        leaving[k] = (
            partial[k, across].astype(jnp.float32) + paired[1, k].astype(jnp.float32)
        ).astype(jnp.bfloat16)
        copy = remote(leaving.at[k], crossed.at[k], rx_send.at[k], rx_recv.at[k], {"tp": across})
        copy.start()
        back_crossing[k] = copy

    def back_send(k):
        back_pairing[0, k].wait_recv()
        back_crossing[k].wait_recv()
        total = partial[k, mine].astype(jnp.float32) + paired[0, k].astype(jnp.float32)
        total = (total + crossed[k].astype(jnp.float32)).astype(jnp.bfloat16)
        if k == 0:
            returned[0] = total
            return
        final[k] = total
        source = (me + n_ep - k) % n_ep
        copy = remote(final.at[k], returned.at[k], rz_send.at[k], rz_recv.at[k], {"ep": source})
        copy.start()
        back_along[k] = copy

    mixer = {}

    def mixer_start():
        get_wo.wait()
        for h in range(heads):
            att[:, h * head : (h + 1) * head] = (run_acc[h] / run_sum[h]).astype(jnp.bfloat16)

        def project(c, carry):
            cols = rows_of(c, col)
            rows = dot_nn(att[...], wo[:, cols]).astype(jnp.bfloat16)
            mixp[:, :, cols] = rows.reshape(n_tp, span // n_tp, col)
            return carry

        lax.fori_loop(0, width // col, project, 0)
        for way, block in ((1, pair_across), (0, pair)):
            copy = remote(
                mixp.at[block], mpaired.at[way], m_send.at[way], m_recv.at[way], {"tp": pair}
            )
            copy.start()
            mixer[way] = copy

    step = 16

    def mixer_cross():
        mixer[1].wait_recv()

        def add_tile(i, carry):
            rows = rows_of(i, step)
            mleaving[rows, :] = (
                mixp[across, rows, :].astype(jnp.float32) + mpaired[1, rows, :].astype(jnp.float32)
            ).astype(jnp.bfloat16)
            return carry

        lax.fori_loop(0, span // n_tp // step, add_tile, 0)
        copy = remote(mleaving, mcrossed, m_send.at[2], m_recv.at[2], {"tp": across})
        copy.start()
        mixer[2] = copy

    def mixer_end():
        mixer[0].wait_recv()
        mixer[2].wait_recv()

        def add_tile(i, carry):
            rows = rows_of(i, step)
            total = mixp[mine, rows, :].astype(jnp.float32) + mpaired[0, rows, :].astype(
                jnp.float32
            )
            mix_ref[rows, :] = (total + mcrossed[rows, :].astype(jnp.float32)).astype(
                jnp.bfloat16
            )
            return carry

        lax.fori_loop(0, span // n_tp // step, add_tile, 0)

    slot_tables(0, own)
    fill_slots(0, 0)
    token_column = jnp.transpose(jnp.broadcast_to(token_key, (8, span)), (1, 0))[:, 0:1]
    for k in range(n_ep):
        base = ((me + k) % n_ep * row_cap).astype(jnp.float32)
        final_hot[:, k * row_cap : (k + 1) * row_cap] = one_hot(
            iota_f32((span, row_cap), 1) + base == token_column
        )
    for k in range(1, n_ep):
        notes_sent[k - 1].wait_recv()
        slot_tables(k, ranks(k))
    pass_on(1)
    kv_step(1)
    relay(1)
    for copy in weights:
        copy.wait()
    fill_slots(1, 1)
    expert_pass((0, 1))
    combine(1, 1)
    combine(0, 0)
    pass_on(2)
    back_cross(1)
    back_cross(0)
    relay(2)
    pass_on(3)
    kv_step(2)
    back_send(1)
    back_send(0)
    relay(3)
    fill_slots(2, 0)
    fill_slots(3, 1)
    expert_pass((2, 3))
    combine(2, 0)
    combine(3, 1)
    back_cross(2)
    back_cross(3)
    kv_step(3)
    mixer_start()
    back_send(2)
    mixer_cross()
    back_send(3)
    for k in range(1, n_ep):
        back_along[k].wait_recv()

    def output_tile(i, carry):
        rows = rows_of(i, 128)
        exp_ref[rows, :] = dot_nn(
            final_hot[rows, :], returned[...].reshape(n_ep * row_cap, quarter)
        ).astype(jnp.bfloat16)
        return carry

    lax.fori_loop(0, span // 128, output_tile, 0)
    mixer_end()

    for copy in notes_sent:
        copy.wait_send()
    for d in range(n_ep - 1):

        @pl.when((me >= d) & (me < n_ep - 1))
        def _():
            kv_copies[d].wait_send()

    for group in (along, crossing, pairing, back_pairing, back_crossing, back_along, mixer):
        for copy in group.values():
            copy.wait_send()


def fused_half(
    queries,
    key_rows,
    value_rows,
    query_gain,
    key_gain,
    log_forget,
    out_weight,
    expert_rows,
    expert_gain,
    routes,
    route_weight,
    gate_weight,
    up_weight,
    down_weight,
    capacity,
):
    n_tp = lax.axis_size("tp")
    n_ep = lax.axis_size("ep")
    span, width = expert_rows.shape
    exp_dev = gate_weight.shape[0]
    hidden = gate_weight.shape[2]
    heads = queries.shape[1] // HEAD_SIZE
    row_cap = exp_dev * capacity // TOP
    part = row_cap // n_tp
    quarter = width // n_tp
    n_slots = exp_dev * capacity
    whole = log_forget.shape[1]
    weight_rows = []
    for j in range(TOP):
        high = lax.reduce_precision(route_weight[j], 8, 7)
        weight_rows += [high, route_weight[j] - high]
    info = jnp.stack(
        [(routes[0] // exp_dev).astype(jnp.float32)]
        + [(routes[j] % exp_dev).astype(jnp.float32) for j in range(TOP)]
        + weight_rows
        + [jnp.zeros((span,), jnp.float32)],
        axis=0,
    )
    low = jnp.bfloat16
    full = jnp.float32
    vmem = pltpu.VMEM
    dma = pltpu.SemaphoreType.DMA
    scratch = [
        vmem((span, heads * HEAD_SIZE), low),
        vmem((span, HEAD_SIZE), low),
        vmem((n_ep, 2, span, HEAD_SIZE), low),
        vmem((1, HEAD_SIZE), full),
        vmem((1, HEAD_SIZE), full),
        vmem((heads, whole), full),
        vmem((heads * HEAD_SIZE, width), low),
        vmem((span, width), low),
        vmem((1, width), full),
        vmem((n_ep, 8, span), full),
        vmem((exp_dev, width, hidden), low),
        vmem((exp_dev, width, hidden), low),
        vmem((exp_dev, hidden, width), low),
        vmem((heads, span, HEAD_SIZE), low),
        vmem((heads, span, 1), full),
        vmem((heads, span, 1), full),
        vmem((heads, span, HEAD_SIZE), full),
        vmem((span, heads * HEAD_SIZE), low),
        vmem((n_tp, span // n_tp, width), low),
        vmem((2, span // n_tp, width), low),
        vmem((span // n_tp, width), low),
        vmem((span // n_tp, width), low),
        vmem((span, width), low),
        vmem((span, span), low),
        vmem((n_ep - 1, part, width), low),
        vmem((n_ep, n_tp, part, width), low),
        vmem((n_ep, n_slots, row_cap), low),
        vmem((n_ep, row_cap, n_slots), low),
        vmem((n_ep, n_slots, 1), full),
        vmem((span, n_ep * row_cap), low),
        vmem((exp_dev, 2 * capacity, width), low),
        vmem((2, exp_dev, capacity, width), low),
        vmem((n_ep, n_tp, row_cap, quarter), low),
        vmem((2, n_ep, row_cap, quarter), low),
        vmem((n_ep, row_cap, quarter), low),
        vmem((n_ep, row_cap, quarter), low),
        vmem((n_ep, row_cap, quarter), low),
        vmem((n_ep, row_cap, quarter), low),
        dma((10,)),
        dma((3, exp_dev)),
        dma((n_ep,)),
        dma((n_ep,)),
        dma((n_ep,)),
        dma((n_ep,)),
        dma((n_ep,)),
        dma((n_ep,)),
        dma((n_ep,)),
        dma((n_ep,)),
        dma((2, n_ep)),
        dma((2, n_ep)),
        dma((2, n_ep)),
        dma((2, n_ep)),
        dma((n_ep,)),
        dma((n_ep,)),
        dma((n_ep,)),
        dma((n_ep,)),
        dma((3,)),
        dma((3,)),
    ]
    return pl.pallas_call(
        functools.partial(fused_kernel, n_ep, n_tp, capacity),
        out_shape=(
            jax.ShapeDtypeStruct((span // n_tp, width), low),
            jax.ShapeDtypeStruct((span, quarter), low),
        ),
        in_specs=[pl.BlockSpec(memory_space=pl.ANY)] * 13,
        out_specs=(
            pl.BlockSpec(memory_space=pltpu.VMEM),
            pl.BlockSpec(memory_space=pltpu.VMEM),
        ),
        scratch_shapes=scratch,
        compiler_params=pltpu.CompilerParams(
            collective_id=0, has_side_effects=True, vmem_limit_bytes=VMEM_LIMIT
        ),
    )(
        queries,
        key_rows,
        value_rows,
        query_gain.reshape(1, -1),
        key_gain.reshape(1, -1),
        log_forget,
        out_weight,
        expert_rows,
        expert_gain.reshape(1, -1),
        info,
        gate_weight,
        up_weight,
        down_weight,
    )


def on_device(
    queries,
    key_rows,
    value_rows,
    query_gain,
    key_gain,
    log_forget,
    out_weight,
    expert_rows,
    expert_gain,
    routes,
    route_weight,
    gate_weight,
    up_weight,
    down_weight,
):
    mixer_args = (
        queries,
        key_rows,
        value_rows,
        query_gain,
        key_gain,
        log_forget,
        out_weight,
    )
    expert_args = (
        expert_rows,
        expert_gain,
        routes,
        route_weight,
        gate_weight,
        up_weight,
        down_weight,
    )
    n_tp = lax.axis_size("tp")
    n_ep = lax.axis_size("ep")
    span = expert_rows.shape[0]
    capacity = n_tp * ((3 * (span // n_tp) * TOP + 2 * EXPERTS - 1) // (2 * EXPERTS))
    fits = (
        n_tp == 4
        and n_ep == 4
        and gate_weight.shape[0] == GROUP_SIZE
        and capacity % 16 == 0
        and key_rows.shape[1] == HEAD_SIZE
    )
    if fits:
        return fused_half(*mixer_args, *expert_args, capacity)
    expert_out = experts_half(*expert_args)
    mixer_part = mixer_half(*mixer_args)
    mixer_out = lax.psum_scatter(mixer_part, "tp", scatter_dimension=0, tiled=True)
    return (mixer_out, expert_out)


def solution(mesh):
    in_specs = (
        P(("grp", "ep"), "tp"),
        P(("grp", "ep"), "tp"),
        P(("grp", "ep"), "tp"),
        P(),
        P(),
        P("tp", "grp"),
        P("tp", None),
        P(("grp", "ep"), None),
        P(),
        P(None, ("grp", "ep")),
        P(None, ("grp", "ep")),
        P("ep", None, "tp"),
        P("ep", None, "tp"),
        P("ep", "tp", None),
    )
    out_specs = (P(("grp", "ep", "tp"), None), P(("grp", "ep"), "tp"))
    return jax.shard_map(
        on_device, mesh=mesh, in_specs=in_specs, out_specs=out_specs, check_vma=False
    )
```

time: 162 us -> 105 us (0.65)
  the two profiles are of different devices: /device:TPU:0 before, /device:TPU:16 now
where the time goes in v1:
time: 105 us; the launch traced here: 104 us
  Pallas kernels  97.2 us (93%)
  local copies, waits for them, and re-layouts  4.39 us (4%)
  other arithmetic  2.26 us (2%)
    pallas_call x1, Pallas kernels, fused_half(): pl.pallas_call(functools.partial(fused_kernel, n_ep, n_tp, capacity), out...  97.2 us
    unnamed x2, local copies, waits for them, and re-layouts  3.75 us

profile of v1, /device:TPU:16, one launch (start us, length us, event | category | flops | bytes accessed | tf_op | source)
XLA Modules:
  0.0 104.5 jit_solution(16025802647392707920)
XLA Ops:
  0.6 0.8 fusion
  1.4 0.7 fusion.3
  2.1 0.8 slice_subtract_fusion
  2.9 0.6 stack.2.info_hbm
  3.5 97.2 %shard_map.149 = (bf16[128,2048]{1,0:T(8,128)(2,1)}, bf16[512,512]{1,0:T(8,128)(2,1)}) custom-call(bf16[512,256]{1,0:T(8,128)(2,1)} %q_hbm.1, bf16[512,128]{1,0:T(8,128)(2,1)} %k_hbm.1, bf16[512,128]{1,0:T(8,128)(2,1)} %v_hbm.1, f32[1,128]{1,0:T(1,128)} %bitcast.4, f32[1,128]{1,0:T(1,128)} %bitcast.5, f32[2,2048]{1,0:T(2,128)} %lf_hbm.1, ...), custom_call_target="tpu_custom_call" | custom-call | tf_op jit(solution)/shard_map/pallas_call | solution.py:839
  100.7 1.9 %copy.18 = bf16[128,2048]{1,0:T(8,128)(2,1)} copy(bf16[128,2048]{1,0:T(8,128)(2,1)} %get-tuple-element.11) | data formatting | bytes 1048576
  102.6 1.9 %copy.19 = bf16[512,512]{1,0:T(8,128)(2,1)} copy(bf16[512,512]{1,0:T(8,128)(2,1)} %get-tuple-element.12) | data formatting | bytes 1048576
  (1 shorter events, 0.0 us)

commit v2 on v1

--- a/solution.py
+++ b/solution.py
@@ -12,6 +12,7 @@
 TOP = 2
 GROUP_SIZE = 8
 VMEM_LIMIT = 65000 * 1024
+PIECES = 2
 
 
 def head_norm(inputs, scale_gain):
@@ -198,7 +199,8 @@
     wo_hbm,
     x_hbm,
     xg_hbm,
-    info_hbm,
+    routes_hbm,
+    share_hbm,
     wg_hbm,
     wu_hbm,
     wd_hbm,
@@ -213,6 +215,8 @@
     wo,
     x_in,
     xg,
+    routes,
+    share,
     info,
     wg,
     wu,
@@ -234,6 +238,7 @@
     return_hot,
     slot_weight,
     final_hot,
+    exp_acc,
     slots,
     down,
     partial,
@@ -277,6 +282,9 @@
     n_slots = exp_dev * capacity
     quarter = width // n_tp
     score_scale = (head**-0.5) * LOG2E
+    near = n_ep - 1 - (n_ep - 2) * (me // (n_ep - 1))
+    middle = 2 - me * (n_ep - 1 - me) // 2
+    order = (near, middle, 2 * n_ep - 2 - near - middle)
 
     fetches = []
 
@@ -289,20 +297,14 @@
     get_k = fetch(k_hbm, k_in)
     get_kg = fetch(kg_hbm, kg)
     get_v = fetch(v_hbm, kv.at[0, 1])
-    get_info = fetch(info_hbm, info.at[0])
+    get_routes = fetch(routes_hbm, routes)
+    get_share = fetch(share_hbm, share)
     get_x = fetch(x_hbm, x_in)
     get_xg = fetch(xg_hbm, xg)
     get_q = fetch(q_hbm, q_in)
     get_qg = fetch(qg_hbm, qg)
     get_lf = fetch(lf_hbm, lf)
     get_wo = fetch(wo_hbm, wo)
-    weights = []
-    for e in range(exp_dev):
-        for i, (src, dst) in enumerate(((wg_hbm, wg), (wu_hbm, wu), (wd_hbm, wd))):
-            copy = pltpu.make_async_copy(src.at[e], dst.at[e], w_sem.at[i, e])
-            copy.start()
-            weights.append(copy)
-
     barrier = pltpu.get_barrier_semaphore()
     peers = [{"ep": (me + k) % n_ep} for k in range(1, n_ep)] + [{"tp": pair}, {"tp": across}]
     for peer in peers:
@@ -316,33 +318,60 @@
         return (rows * factor * gain).astype(jnp.bfloat16)
 
     kv[0, 0] = norm_heads(k_in[...].astype(jnp.float32), kg[...])
-    get_info.wait()
+    get_routes.wait()
+    get_share.wait()
     get_v.wait()
+    chosen_ids = routes[...].astype(jnp.float32)
+    shares = share[...]
+    high = shares.astype(jnp.bfloat16).astype(jnp.float32)
+    group = jnp.zeros((1, span), jnp.float32)
+    for d in range(1, n_ep):
+        group = group + jnp.where(chosen_ids[0:1] >= float(d * exp_dev), 1.0, 0.0)
+    kinds = iota_f32((8, span), 0)
+    entries = [group] + [chosen_ids[j : j + 1] - group * exp_dev for j in range(TOP)]
+    for j in range(TOP):
+        entries += [high[j : j + 1], shares[j : j + 1] - high[j : j + 1]]
+    table = jnp.zeros((8, span), jnp.float32)
+    for i, entry in enumerate(entries):
+        table = jnp.where(kinds == float(i), entry, table)
+    info[0] = table
     pl.semaphore_wait(barrier, len(peers))
+
+    kv_copies = [
+        [
+            remote(
+                kv.at[d, i],
+                kv.at[d + 1, i],
+                kv_send.at[d, i],
+                kv_recv.at[d + 1, i],
+                {"ep": (me + 1) % n_ep},
+            )
+            for i in range(2)
+        ]
+        for d in range(n_ep - 1)
+    ]
+
+    def kv_pass(d, i):
+        @pl.when((me >= d) & (me < n_ep - 1))
+        def _():
+            kv_copies[d][i].start()
+
+    kv_pass(0, 0)
+
+    @pl.when(me == 0)
+    def _():
+        kv_copies[0][1].start()
 
     notes_sent = []
     for k in range(1, n_ep):
         copy = remote(
-            info_hbm, info.at[k], i_send.at[k], i_recv.at[k], {"ep": (me + k) % n_ep}
+            info.at[0], info.at[k], i_send.at[k], i_recv.at[k], {"ep": (me + k) % n_ep}
         )
         copy.start()
         notes_sent.append(copy)
 
-    kv_copies = [
-        remote(kv.at[d], kv.at[d + 1], kv_send.at[d], kv_recv.at[d + 1], {"ep": (me + 1) % n_ep})
-        for d in range(n_ep - 1)
-    ]
-
-    def kv_pass(d):
-        @pl.when((me >= d) & (me < n_ep - 1))
-        def _():
-            kv_copies[d].start()
-
-    kv_pass(0)
-
     me_f = me.astype(jnp.float32)
     earlier[...] = one_hot(iota_f32((span, span), 0) < iota_f32((span, span), 1))
-    kinds = iota_f32((8, span), 0)
 
     def ranks(k):
         table = info[k]
@@ -395,6 +424,13 @@
 
     get_x.wait()
     get_xg.wait()
+    weights = []
+    for e in range(exp_dev):
+        for i, (src, dst) in enumerate(((wg_hbm, wg), (wu_hbm, wu), (wd_hbm, wd))):
+            copy = pltpu.make_async_copy(src.at[e], dst.at[e], w_sem.at[i, e])
+            copy.start()
+            weights.append(copy)
+
     norm_rows = 32
 
     def norm_tile(i, carry):
@@ -402,15 +438,15 @@
         normed[rows, :] = norm_heads(x_in[rows, :].astype(jnp.float32), xg[...])
         return carry
 
-    lax.fori_loop(0, span // norm_rows, norm_tile, 0)
+    lax.fori_loop(0, span // norm_rows, norm_tile, 0, unroll=2)
     own = ranks(0)
     _, dest, _, _, rank, _ = own
     token_key = dest * row_cap + rank
     part_base = (mine * part).astype(jnp.float32)
     part_rows = iota_f32((part, span), 0) + part_base
     chosen = []
-    for k in range(1, n_ep):
-        base = ((me + k) % n_ep * row_cap).astype(jnp.float32)
+    for k in order:
+        base = ((me + n_ep - k) % n_ep * row_cap).astype(jnp.float32)
         chosen.append(jnp.where(part_rows + base == token_key, 1.0, 0.0))
     chosen = jnp.concatenate(chosen, axis=0).astype(jnp.bfloat16)
     col = 256
@@ -418,22 +454,22 @@
     def send_tile(i, carry):
         cols = rows_of(i, col)
         rows = dot_nn(chosen, normed[:, cols]).astype(jnp.bfloat16)
-        for k in range(1, n_ep):
-            send_rows[k - 1, :, cols] = rows[(k - 1) * part : k * part]
+        for p in range(n_ep - 1):
+            send_rows[p, :, cols] = rows[p * part : (p + 1) * part]
         return carry
 
-    lax.fori_loop(0, width // col, send_tile, 0)
-    along = {}
-    for k in range(1, n_ep):
+    lax.fori_loop(0, width // col, send_tile, 0, unroll=2)
+    along = []
+    for p, k in enumerate(order):
         copy = remote(
-            send_rows.at[k - 1],
-            arrived.at[k, mine],
-            z_send.at[k],
-            z_recv.at[k],
-            {"ep": (me + k) % n_ep},
+            send_rows.at[p],
+            arrived.at[n_ep - k, mine],
+            z_send.at[n_ep - k],
+            z_recv.at[n_ep - k],
+            {"ep": (me + n_ep - k) % n_ep},
         )
         copy.start()
-        along[k] = copy
+        along.append(copy)
 
     own_rows = one_hot(
         iota_f32((row_cap, span), 0) + (me * row_cap).astype(jnp.float32) == token_key
@@ -446,7 +482,7 @@
             arrived[0, p, :, cols] = rows[p * part : (p + 1) * part]
         return carry
 
-    lax.fori_loop(0, width // col, own_tile, 0)
+    lax.fori_loop(0, width // col, own_tile, 0, unroll=2)
 
     get_q.wait()
     get_qg.wait()
@@ -491,46 +527,61 @@
                     )
                 return carry
 
-            lax.fori_loop(0, span // tile, query_tile, 0)
-
-    attend(0)
-
-    def kv_step(d):
-        @pl.when(me >= d)
-        def _():
-            kv_copies[d - 1].wait_recv()
-
-        if d < n_ep - 1:
-            kv_pass(d)
-
+            lax.fori_loop(0, span // tile, query_tile, 0, unroll=2)
+
+    def kv_forward(d):
+        for i in range(2):
+
+            @pl.when(me >= d)
+            def _():
+                kv_copies[d - 1][i].wait_recv()
+
+            if d < n_ep - 1:
+                kv_pass(d, i)
+
+    def kv_attend(d):
         @pl.when(me >= d)
         def _():
             attend(d)
 
-    crossing = {}
-    pairing = {}
-
-    def pass_on(k):
-        along[k].wait_recv()
+    inner = (me > 0) & (me < n_ep - 1)
+    arrivals = []
+    crossing = []
+    pairing = []
+    for k in order:
         place = arrived.at[k, mine]
-        copy = remote(place, place, x_send.at[k], x_recv.at[k], {"tp": across})
-        copy.start()
-        crossing[k] = copy
-        copy = remote(place, place, c_send.at[0, k], c_recv.at[0, k], {"tp": pair})
-        copy.start()
-        pairing[0, k] = copy
-
-    def relay(k):
-        crossing[k].wait_recv()
-        place = arrived.at[k, across]
-        copy = remote(place, place, c_send.at[1, k], c_recv.at[1, k], {"tp": pair})
-        copy.start()
-        pairing[1, k] = copy
-
-    def fill_slots(k, side):
-        if k > 0:
-            pairing[0, k].wait_recv()
-            pairing[1, k].wait_recv()
+        relayed = arrived.at[k, across]
+        arrivals.append(
+            remote(place, place, z_send.at[k], z_recv.at[k], {"ep": (me + k) % n_ep})
+        )
+        crossing.append(remote(place, place, x_send.at[k], x_recv.at[k], {"tp": across}))
+        pairing.append(
+            [
+                remote(block, block, c_send.at[i, k], c_recv.at[i, k], {"tp": pair})
+                for i, block in enumerate((place, relayed))
+            ]
+        )
+
+    def only(condition, *steps):
+        @pl.when(condition)
+        def _():
+            for step in steps:
+                step[0](*step[1:])
+
+    def pass_on(p):
+        arrivals[p].wait_recv()
+        crossing[p].start()
+        pairing[p][0].start()
+
+    def relay(p):
+        crossing[p].wait_recv()
+        pairing[p][1].start()
+
+    def fill_slots(p, side):
+        k = 0 if p is None else order[p]
+        if p is not None:
+            pairing[p][0].wait_recv()
+            pairing[p][1].wait_recv()
 
         def slot_tile(i, carry):
             cols = rows_of(i, col)
@@ -542,42 +593,48 @@
                 ]
             return carry
 
-        lax.fori_loop(0, width // col, slot_tile, 0)
+        lax.fori_loop(0, width // col, slot_tile, 0, unroll=2)
 
     wide = 512
 
-    def expert_pass(sources):
+    def expert_pass(sources, first_side, low, high):
+        sides = slice(first_side * capacity, (first_side + len(sources)) * capacity)
+
         def one_expert(e, carry):
-            rows = slots[e]
+            rows = slots[e, sides]
             gate_part = dot_nn(rows, wg[e])
             up_part = dot_nn(rows, wu[e])
             weight = jnp.concatenate(
-                [slot_weight[k, rows_of(e, capacity), :] for k in sources], axis=0
+                [
+                    slot_weight[0 if p is None else order[p], rows_of(e, capacity), :]
+                    for p in sources
+                ], axis=0
             )
             hidden = gate_part / (1.0 + jnp.exp(-gate_part)) * up_part * weight
             hidden = hidden.astype(jnp.bfloat16)
             for c in range(width // wide):
                 cols = slice(c * wide, (c + 1) * wide)
                 result = dot_nn(hidden, wd[e, :, cols]).astype(jnp.bfloat16)
-                for side in range(len(sources)):
-                    down[side, e, :, cols] = result[side * capacity : (side + 1) * capacity]
+                for i in range(len(sources)):
+                    down[first_side + i, e, :, cols] = result[i * capacity : (i + 1) * capacity]
             return carry
 
-        lax.fori_loop(0, exp_dev, one_expert, 0)
+        lax.fori_loop(low, high, one_expert, 0, unroll=2)
 
     back_pairing = {}
     back_crossing = {}
     back_along = {}
-    order = list(range(1, n_ep)) + [0]
-
-    def combine(k, side):
+
+    def combine(p, side):
+        k = 0 if p is None else order[p]
+
         def combine_tile(c, carry):
             cols = rows_of(c, quarter)
             rows = down[side, :, :, cols].reshape(n_slots, quarter)
             partial[k, c] = dot_nn(return_hot[k], rows).astype(jnp.bfloat16)
             return carry
 
-        lax.fori_loop(0, n_tp, combine_tile, 0)
+        lax.fori_loop(0, n_tp, combine_tile, 0, unroll=2)
         for way, block in ((1, pair_across), (0, pair)):
             copy = remote(
                 partial.at[k, block],
@@ -587,35 +644,66 @@
                 {"tp": pair},
             )
             copy.start()
-            back_pairing[way, k] = copy
-
-    def back_cross(k):
-        back_pairing[1, k].wait_recv()
-        leaving[k] = (
-            partial[k, across].astype(jnp.float32) + paired[1, k].astype(jnp.float32)
+            back_pairing[way, p] = copy
+
+    rows_half = row_cap // 2
+
+    def back_cross(p, h):
+        k = 0 if p is None else order[p]
+        if h == 0:
+            back_pairing[1, p].wait_recv()
+        rows = slice(h * rows_half, (h + 1) * rows_half)
+        leaving[k, rows] = (
+            partial[k, across, rows].astype(jnp.float32) + paired[1, k, rows].astype(jnp.float32)
         ).astype(jnp.bfloat16)
-        copy = remote(leaving.at[k], crossed.at[k], rx_send.at[k], rx_recv.at[k], {"tp": across})
-        copy.start()
-        back_crossing[k] = copy
-
-    def back_send(k):
-        back_pairing[0, k].wait_recv()
-        back_crossing[k].wait_recv()
-        total = partial[k, mine].astype(jnp.float32) + paired[0, k].astype(jnp.float32)
-        total = (total + crossed[k].astype(jnp.float32)).astype(jnp.bfloat16)
-        if k == 0:
-            returned[0] = total
+        back_crossing[p, h].start()
+
+    def back_send(p, h):
+        k = 0 if p is None else order[p]
+        if h == 0:
+            back_pairing[0, p].wait_recv()
+        back_crossing[p, h].wait_recv()
+        rows = slice(h * rows_half, (h + 1) * rows_half)
+        total = partial[k, mine, rows].astype(jnp.float32) + paired[0, k, rows].astype(jnp.float32)
+        total = (total + crossed[k, rows].astype(jnp.float32)).astype(jnp.bfloat16)
+        if p is None:
+            returned[0, rows] = total
             return
-        final[k] = total
-        source = (me + n_ep - k) % n_ep
-        copy = remote(final.at[k], returned.at[k], rz_send.at[k], rz_recv.at[k], {"ep": source})
-        copy.start()
-        back_along[k] = copy
-
-    mixer = {}
+        final[k, rows] = total
+        back_along[p, h].start()
+
+    for p in (None, 0, 1, 2):
+        k = 0 if p is None else order[p]
+        for h in range(2):
+            rows = pl.ds(h * rows_half, rows_half)
+            back_crossing[p, h] = remote(
+                leaving.at[k, rows],
+                crossed.at[k, rows],
+                rx_send.at[k, h],
+                rx_recv.at[k, h],
+                {"tp": across},
+            )
+            if p is not None:
+                back_along[p, h] = remote(
+                    final.at[k, rows],
+                    returned.at[k, rows],
+                    rz_send.at[k, h],
+                    rz_recv.at[k, h],
+                    {"ep": (me + n_ep - k) % n_ep},
+                )
+
+    mixer_copies = {
+        way: remote(mixp.at[block], mpaired.at[way], m_send.at[way], m_recv.at[way], {"tp": pair})
+        for way, block in ((1, pair_across), (0, pair))
+    }
+    half = span // n_tp // 2
+    for h in range(2):
+        block = slice(h * half, (h + 1) * half)
+        mixer_copies[2 + h] = remote(
+            mleaving.at[block], mcrossed.at[block], m_send.at[2 + h], m_recv.at[2 + h], {"tp": across}
+        )
 
     def mixer_start():
-        get_wo.wait()
         for h in range(heads):
             att[:, h * head : (h + 1) * head] = (run_acc[h] / run_sum[h]).astype(jnp.bfloat16)
 
@@ -625,34 +713,30 @@
             mixp[:, :, cols] = rows.reshape(n_tp, span // n_tp, col)
             return carry
 
-        lax.fori_loop(0, width // col, project, 0)
-        for way, block in ((1, pair_across), (0, pair)):
-            copy = remote(
-                mixp.at[block], mpaired.at[way], m_send.at[way], m_recv.at[way], {"tp": pair}
-            )
-            copy.start()
-            mixer[way] = copy
+        lax.fori_loop(0, width // col, project, 0, unroll=2)
+        mixer_copies[1].start()
+        mixer_copies[0].start()
 
     step = 16
 
-    def mixer_cross():
-        mixer[1].wait_recv()
+    def mixer_cross(h):
+        if h == 0:
+            mixer_copies[1].wait_recv()
 
         def add_tile(i, carry):
-            rows = rows_of(i, step)
+            rows = pl.ds(pl.multiple_of(h * half + i * step, step), step)
             mleaving[rows, :] = (
                 mixp[across, rows, :].astype(jnp.float32) + mpaired[1, rows, :].astype(jnp.float32)
             ).astype(jnp.bfloat16)
             return carry
 
-        lax.fori_loop(0, span // n_tp // step, add_tile, 0)
-        copy = remote(mleaving, mcrossed, m_send.at[2], m_recv.at[2], {"tp": across})
-        copy.start()
-        mixer[2] = copy
+        lax.fori_loop(0, half // step, add_tile, 0)
+        mixer_copies[2 + h].start()
 
     def mixer_end():
-        mixer[0].wait_recv()
-        mixer[2].wait_recv()
+        mixer_copies[0].wait_recv()
+        mixer_copies[2].wait_recv()
+        mixer_copies[3].wait_recv()
 
         def add_tile(i, carry):
             rows = rows_of(i, step)
@@ -666,58 +750,94 @@
 
         lax.fori_loop(0, span // n_tp // step, add_tile, 0)
 
+    outer = jnp.logical_not(inner)
+    last = n_ep - 1
+    attend(0)
+    get_wo.wait()
+    only(me == 0, (mixer_start,))
     slot_tables(0, own)
-    fill_slots(0, 0)
+    fill_slots(None, 0)
+    pass_on(0)
+    for k in range(1, n_ep):
+        notes_sent[k - 1].wait_recv()
+        slot_tables(k, ranks(k))
+    only(inner, (kv_copies[0][1].start,))
+    for copy in weights:
+        copy.wait()
+    split = exp_dev // 2
+    expert_pass((None,), 0, 0, split)
+    relay(0)
+    only(inner, (pass_on, 1))
+    only(me == 0, (mixer_cross, 0))
+    expert_pass((None,), 0, split, exp_dev)
+    combine(None, 0)
+    fill_slots(0, 1)
+    back_cross(None, 0)
+    back_cross(None, 1)
+    only(me == 1, (kv_forward, 1))
+    only(inner, (pass_on, 2))
+    expert_pass((0,), 1, 0, split)
+    only(outer, (pass_on, 1))
+    only(inner, (relay, 1))
+    expert_pass((0,), 1, split, exp_dev)
+    combine(0, 1)
+    only(outer, (pass_on, 2))
+    only(me > 1, (kv_forward, 1))
+    only(inner, (back_cross, 0, 0), (back_cross, 0, 1))
+    only(me > 0, (attend, 1))
+    only(outer, (relay, 1))
+    only(inner, (relay, 2))
+    fill_slots(1, 0)
+    only(me == 0, (mixer_cross, 1))
+    only(me == 1, (mixer_start,))
+    only(me > 1, (kv_forward, 2), (attend, 2))
+    only(outer, (relay, 2), (back_cross, 0, 0), (back_cross, 0, 1))
+    only(me == 1, (mixer_cross, 0))
+    fill_slots(2, 1)
+    expert_pass((1, 2), 0, 0, split)
+    only(inner, (back_send, 0, 0), (back_send, 0, 1))
+    expert_pass((1, 2), 0, split, exp_dev)
+    only(outer, (back_send, 0, 0), (back_send, 0, 1))
+    combine(1, 0)
+    combine(2, 1)
+    back_cross(1, 0)
+    back_cross(1, 1)
+    only(me == 3, (kv_forward, 3), (attend, 3))
+    only(me > 1, (mixer_start,))
+    back_send(1, 0)
+    back_cross(2, 0)
+    back_send(1, 1)
+    back_cross(2, 1)
+    back_send(None, 0)
+    back_send(None, 1)
+    only(me > 1, (mixer_cross, 0))
+    back_send(2, 0)
+    back_send(2, 1)
+    only(me > 0, (mixer_cross, 1))
     token_column = jnp.transpose(jnp.broadcast_to(token_key, (8, span)), (1, 0))[:, 0:1]
     for k in range(n_ep):
         base = ((me + k) % n_ep * row_cap).astype(jnp.float32)
-        final_hot[:, k * row_cap : (k + 1) * row_cap] = one_hot(
+        final_hot[k] = one_hot(
             iota_f32((span, row_cap), 1) + base == token_column
         )
-    for k in range(1, n_ep):
-        notes_sent[k - 1].wait_recv()
-        slot_tables(k, ranks(k))
-    pass_on(1)
-    kv_step(1)
-    relay(1)
-    for copy in weights:
-        copy.wait()
-    fill_slots(1, 1)
-    expert_pass((0, 1))
-    combine(1, 1)
-    combine(0, 0)
-    pass_on(2)
-    back_cross(1)
-    back_cross(0)
-    relay(2)
-    pass_on(3)
-    kv_step(2)
-    back_send(1)
-    back_send(0)
-    relay(3)
-    fill_slots(2, 0)
-    fill_slots(3, 1)
-    expert_pass((2, 3))
-    combine(2, 0)
-    combine(3, 1)
-    back_cross(2)
-    back_cross(3)
-    kv_step(3)
-    mixer_start()
-    back_send(2)
-    mixer_cross()
-    back_send(3)
-    for k in range(1, n_ep):
-        back_along[k].wait_recv()
-
-    def output_tile(i, carry):
-        rows = rows_of(i, 128)
-        exp_ref[rows, :] = dot_nn(
-            final_hot[rows, :], returned[...].reshape(n_ep * row_cap, quarter)
-        ).astype(jnp.bfloat16)
-        return carry
-
-    lax.fori_loop(0, span // 128, output_tile, 0)
+    for p in (None, 0, 1, 2):
+        k = 0 if p is None else order[p]
+        if p is not None:
+            for h in range(2):
+                back_along[p, h].wait_recv()
+
+        def output_tile(i, carry):
+            rows = rows_of(i, 128)
+            total = dot_nn(final_hot[k, rows, :], returned[k])
+            if p is not None:
+                total = total + exp_acc[rows, :]
+            if p == n_ep - 2:
+                exp_ref[rows, :] = total.astype(jnp.bfloat16)
+            else:
+                exp_acc[rows, :] = total
+            return carry
+
+        lax.fori_loop(0, span // 128, output_tile, 0, unroll=2)
     mixer_end()
 
     for copy in notes_sent:
@@ -726,9 +846,12 @@
 
         @pl.when((me >= d) & (me < n_ep - 1))
         def _():
-            kv_copies[d].wait_send()
-
-    for group in (along, crossing, pairing, back_pairing, back_crossing, back_along, mixer):
+            for copy in kv_copies[d]:
+                copy.wait_send()
+
+    for copy in along + crossing + pairing[0] + pairing[1] + pairing[2]:
+        copy.wait_send()
+    for group in (back_pairing, back_crossing, back_along, mixer_copies):
         for copy in group.values():
             copy.wait_send()
 
@@ -761,17 +884,6 @@
     quarter = width // n_tp
     n_slots = exp_dev * capacity
     whole = log_forget.shape[1]
-    weight_rows = []
-    for j in range(TOP):
-        high = lax.reduce_precision(route_weight[j], 8, 7)
-        weight_rows += [high, route_weight[j] - high]
-    info = jnp.stack(
-        [(routes[0] // exp_dev).astype(jnp.float32)]
-        + [(routes[j] % exp_dev).astype(jnp.float32) for j in range(TOP)]
-        + weight_rows
-        + [jnp.zeros((span,), jnp.float32)],
-        axis=0,
-    )
     low = jnp.bfloat16
     full = jnp.float32
     vmem = pltpu.VMEM
@@ -786,6 +898,8 @@
         vmem((heads * HEAD_SIZE, width), low),
         vmem((span, width), low),
         vmem((1, width), full),
+        vmem((TOP, span), jnp.int32),
+        vmem((TOP, span), full),
         vmem((n_ep, 8, span), full),
         vmem((exp_dev, width, hidden), low),
         vmem((exp_dev, width, hidden), low),
@@ -806,7 +920,8 @@
         vmem((n_ep, n_slots, row_cap), low),
         vmem((n_ep, row_cap, n_slots), low),
         vmem((n_ep, n_slots, 1), full),
-        vmem((span, n_ep * row_cap), low),
+        vmem((n_ep, span, row_cap), low),
+        vmem((span, quarter), full),
         vmem((exp_dev, 2 * capacity, width), low),
         vmem((2, exp_dev, capacity, width), low),
         vmem((n_ep, n_tp, row_cap, quarter), low),
@@ -815,10 +930,10 @@
         vmem((n_ep, row_cap, quarter), low),
         vmem((n_ep, row_cap, quarter), low),
         vmem((n_ep, row_cap, quarter), low),
-        dma((10,)),
+        dma((11,)),
         dma((3, exp_dev)),
-        dma((n_ep,)),
-        dma((n_ep,)),
+        dma((n_ep, 2)),
+        dma((n_ep, 2)),
         dma((n_ep,)),
         dma((n_ep,)),
         dma((n_ep,)),
@@ -829,20 +944,20 @@
         dma((2, n_ep)),
         dma((2, n_ep)),
         dma((2, n_ep)),
-        dma((n_ep,)),
-        dma((n_ep,)),
-        dma((n_ep,)),
-        dma((n_ep,)),
-        dma((3,)),
-        dma((3,)),
+        dma((n_ep, 2)),
+        dma((n_ep, 2)),
+        dma((n_ep, 2)),
+        dma((n_ep, 2)),
+        dma((4,)),
+        dma((4,)),
     ]
-    return pl.pallas_call(
+    mixed, combined = pl.pallas_call(
         functools.partial(fused_kernel, n_ep, n_tp, capacity),
         out_shape=(
             jax.ShapeDtypeStruct((span // n_tp, width), low),
             jax.ShapeDtypeStruct((span, quarter), low),
         ),
-        in_specs=[pl.BlockSpec(memory_space=pl.ANY)] * 13,
+        in_specs=[pl.BlockSpec(memory_space=pl.ANY)] * 14,
         out_specs=(
             pl.BlockSpec(memory_space=pltpu.VMEM),
             pl.BlockSpec(memory_space=pltpu.VMEM),
@@ -861,11 +976,49 @@
         out_weight,
         expert_rows,
         expert_gain.reshape(1, -1),
-        info,
+        routes,
+        route_weight,
         gate_weight,
         up_weight,
         down_weight,
     )
+    return settle(mixed, combined)
+
+
+def settle_kernel(first_in, second_in, first_out, second_out, first, second, sems):
+    loads = []
+    for i, (src, dst) in enumerate(((first_in, first), (second_in, second))):
+        rows = dst.shape[0] // PIECES
+        for c in range(PIECES):
+            piece = pl.ds(c * rows, rows)
+            copy = pltpu.make_async_copy(src.at[piece], dst.at[piece], sems.at[0, i, c])
+            copy.start()
+            loads.append((i, c, piece, copy))
+    stores = []
+    for i, c, piece, load in loads:
+        load.wait()
+        src, dst = ((first, first_out), (second, second_out))[i]
+        copy = pltpu.make_async_copy(src.at[piece], dst.at[piece], sems.at[1, i, c])
+        copy.start()
+        stores.append(copy)
+    for copy in stores:
+        copy.wait()
+
+
+def settle(first, second):
+    anywhere = pl.BlockSpec(memory_space=pltpu.HBM)
+    return pl.pallas_call(
+        settle_kernel,
+        out_shape=tuple(jax.ShapeDtypeStruct(a.shape, a.dtype) for a in (first, second)),
+        in_specs=[anywhere, anywhere],
+        out_specs=(anywhere, anywhere),
+        scratch_shapes=[
+            pltpu.VMEM(first.shape, first.dtype),
+            pltpu.VMEM(second.shape, second.dtype),
+            pltpu.SemaphoreType.DMA((2, 2, PIECES)),
+        ],
+        compiler_params=pltpu.CompilerParams(vmem_limit_bytes=VMEM_LIMIT),
+    )(first, second)
 
 
 def on_device(

time: 105 us -> 76.9 us (0.73)
  the two profiles are of different devices: /device:TPU:16 before, /device:TPU:0 now
where the time goes in v2:
time: 76.9 us; the launch traced here: 76.7 us
  Pallas kernels  75.9 us (99%)
  between operations  0.8 us (1%)
    pallas_call x1, Pallas kernels, fused_half(): pl.pallas_call(functools.partial(fused_kernel, n_ep, n_tp, capacity), out...  73.9 us
    pallas_call x1, Pallas kernels, settle(): pl.pallas_call(settle_kernel, out_shape=tuple((jax.ShapeDtypeStruct(a.sha...  1.98 us

profile of v2, /device:TPU:0, one launch (start us, length us, event | category | flops | bytes accessed | tf_op | source)
XLA Modules:
  0.0 76.7 jit_solution(2265929369142423665)
XLA Ops:
  0.6 73.9 %shard_map.149 = (bf16[128,2048]{1,0:T(8,128)(2,1)}, bf16[512,512]{1,0:T(8,128)(2,1)}) custom-call(bf16[512,256]{1,0:T(8,128)(2,1)} %q_hbm.1, bf16[512,128]{1,0:T(8,128)(2,1)} %k_hbm.1, bf16[512,128]{1,0:T(8,128)(2,1)} %v_hbm.1, f32[1,128]{1,0:T(1,128)} %bitcast.4, f32[1,128]{1,0:T(1,128)} %bitcast.5, f32[2,2048]{1,0:T(2,128)} %lf_hbm.1, ...), custom_call_target="tpu_custom_call" | custom-call | tf_op jit(solution)/shard_map/pallas_call | solution.py:954
  74.6 2.0 %shard_map.150 = (bf16[128,2048]{1,0:T(8,128)(2,1)}, bf16[512,512]{1,0:T(8,128)(2,1)}) custom-call(bf16[128,2048]{1,0:T(8,128)(2,1)} %get-tuple-element.4.first_in, bf16[512,512]{1,0:T(8,128)(2,1)} %get-tuple-element.5.second_in), custom_call_target="tpu_custom_call" | custom-call | tf_op jit(solution)/shard_map/pallas_call | solution.py:1010

commit v3 on v2

--- a/solution.py
+++ b/solution.py
@@ -204,6 +204,8 @@
     wg_hbm,
     wu_hbm,
     wd_hbm,
+    mix_hbm,
+    exp_hbm,
     mix_ref,
     exp_ref,
     q_in,
@@ -213,7 +215,7 @@
     kg,
     lf,
     wo,
-    x_in,
+    mixp,
     xg,
     routes,
     share,
@@ -226,9 +228,7 @@
     run_sum,
     run_acc,
     att,
-    mixp,
     mpaired,
-    mleaving,
     mcrossed,
     normed,
     earlier,
@@ -243,9 +243,7 @@
     down,
     partial,
     paired,
-    leaving,
     crossed,
-    final,
     returned,
     in_sem,
     w_sem,
@@ -267,18 +265,22 @@
     rz_recv,
     m_send,
     m_recv,
+    out_sem,
 ):
     me = lax.axis_index("ep")
     mine = lax.axis_index("tp")
     pair = mine + 1 - 2 * (mine % 2)
     across = (mine + n_tp // 2) % n_tp
     pair_across = (pair + n_tp // 2) % n_tp
-    span, width = x_in.shape
+    span, width = x_hbm.shape
+    block_rows = span // n_tp
     heads = q_norm.shape[0]
     head = q_norm.shape[2]
     exp_dev = wg.shape[0]
     part = send_rows.shape[1]
     row_cap = part * n_tp
+    lead = (part + 31) // 32 * 16
+    chunks = (pl.ds(0, lead), pl.ds(lead, part - lead))
     n_slots = exp_dev * capacity
     quarter = width // n_tp
     score_scale = (head**-0.5) * LOG2E
@@ -299,7 +301,7 @@
     get_v = fetch(v_hbm, kv.at[0, 1])
     get_routes = fetch(routes_hbm, routes)
     get_share = fetch(share_hbm, share)
-    get_x = fetch(x_hbm, x_in)
+    get_x = [fetch(x_hbm.at[pl.ds(i * block_rows, block_rows)], mixp.at[i]) for i in range(n_tp)]
     get_xg = fetch(xg_hbm, xg)
     get_q = fetch(q_hbm, q_in)
     get_qg = fetch(qg_hbm, qg)
@@ -422,7 +424,8 @@
         return_hot[k] = (lane_hits[0] + lane_hits[1]).astype(jnp.bfloat16)
         slot_weight[k] = jnp.sum(gains, axis=1, keepdims=True)
 
-    get_x.wait()
+    for copy in get_x:
+        copy.wait()
     get_xg.wait()
     weights = []
     for e in range(exp_dev):
@@ -435,7 +438,9 @@
 
     def norm_tile(i, carry):
         rows = rows_of(i, norm_rows)
-        normed[rows, :] = norm_heads(x_in[rows, :].astype(jnp.float32), xg[...])
+        per = block_rows // norm_rows
+        source = mixp[i // per, rows_of(i % per, norm_rows), :]
+        normed[rows, :] = norm_heads(source.astype(jnp.float32), xg[...])
         return carry
 
     lax.fori_loop(0, span // norm_rows, norm_tile, 0, unroll=2)
@@ -461,15 +466,16 @@
     lax.fori_loop(0, width // col, send_tile, 0, unroll=2)
     along = []
     for p, k in enumerate(order):
-        copy = remote(
-            send_rows.at[p],
-            arrived.at[n_ep - k, mine],
-            z_send.at[n_ep - k],
-            z_recv.at[n_ep - k],
-            {"ep": (me + n_ep - k) % n_ep},
-        )
-        copy.start()
-        along.append(copy)
+        for h, rows in enumerate(chunks):
+            copy = remote(
+                send_rows.at[p, rows],
+                arrived.at[n_ep - k, mine, rows],
+                z_send.at[n_ep - k, h],
+                z_recv.at[n_ep - k, h],
+                {"ep": (me + n_ep - k) % n_ep},
+            )
+            copy.start()
+            along.append(copy)
 
     own_rows = one_hot(
         iota_f32((row_cap, span), 0) + (me * row_cap).astype(jnp.float32) == token_key
@@ -549,18 +555,21 @@
     crossing = []
     pairing = []
     for k in order:
-        place = arrived.at[k, mine]
-        relayed = arrived.at[k, across]
-        arrivals.append(
-            remote(place, place, z_send.at[k], z_recv.at[k], {"ep": (me + k) % n_ep})
-        )
-        crossing.append(remote(place, place, x_send.at[k], x_recv.at[k], {"tp": across}))
-        pairing.append(
-            [
-                remote(block, block, c_send.at[i, k], c_recv.at[i, k], {"tp": pair})
-                for i, block in enumerate((place, relayed))
-            ]
-        )
+        for h, rows in enumerate(chunks):
+            place = arrived.at[k, mine, rows]
+            relayed = arrived.at[k, across, rows]
+            arrivals.append(
+                remote(place, place, z_send.at[k, h], z_recv.at[k, h], {"ep": (me + k) % n_ep})
+            )
+            crossing.append(
+                remote(place, place, x_send.at[k, h], x_recv.at[k, h], {"tp": across})
+            )
+            pairing.append(
+                [
+                    remote(block, block, c_send.at[i, k, h], c_recv.at[i, k, h], {"tp": pair})
+                    for i, block in enumerate((place, relayed))
+                ]
+            )
 
     def only(condition, *steps):
         @pl.when(condition)
@@ -568,20 +577,21 @@
             for step in steps:
                 step[0](*step[1:])
 
-    def pass_on(p):
-        arrivals[p].wait_recv()
-        crossing[p].start()
-        pairing[p][0].start()
-
-    def relay(p):
-        crossing[p].wait_recv()
-        pairing[p][1].start()
+    def pass_on(p, h):
+        arrivals[2 * p + h].wait_recv()
+        crossing[2 * p + h].start()
+        pairing[2 * p + h][0].start()
+
+    def relay(p, h):
+        crossing[2 * p + h].wait_recv()
+        pairing[2 * p + h][1].start()
 
     def fill_slots(p, side):
         k = 0 if p is None else order[p]
         if p is not None:
-            pairing[p][0].wait_recv()
-            pairing[p][1].wait_recv()
+            for h in range(2):
+                pairing[2 * p + h][0].wait_recv()
+                pairing[2 * p + h][1].wait_recv()
 
         def slot_tile(i, carry):
             cols = rows_of(i, col)
@@ -628,23 +638,17 @@
     def combine(p, side):
         k = 0 if p is None else order[p]
 
-        def combine_tile(c, carry):
+        def block(c):
             cols = rows_of(c, quarter)
             rows = down[side, :, :, cols].reshape(n_slots, quarter)
             partial[k, c] = dot_nn(return_hot[k], rows).astype(jnp.bfloat16)
-            return carry
-
-        lax.fori_loop(0, n_tp, combine_tile, 0, unroll=2)
-        for way, block in ((1, pair_across), (0, pair)):
-            copy = remote(
-                partial.at[k, block],
-                paired.at[way, k],
-                rc_send.at[way, k],
-                rc_recv.at[way, k],
-                {"tp": pair},
-            )
-            copy.start()
-            back_pairing[way, p] = copy
+
+        block(pair_across)
+        block(pair)
+        back_pairing[1, p].start()
+        back_pairing[0, p].start()
+        block(across)
+        block(mine)
 
     rows_half = row_cap // 2
 
@@ -653,7 +657,7 @@
         if h == 0:
             back_pairing[1, p].wait_recv()
         rows = slice(h * rows_half, (h + 1) * rows_half)
-        leaving[k, rows] = (
+        partial[k, across, rows] = (
             partial[k, across, rows].astype(jnp.float32) + paired[1, k, rows].astype(jnp.float32)
         ).astype(jnp.bfloat16)
         back_crossing[p, h].start()
@@ -669,15 +673,23 @@
         if p is None:
             returned[0, rows] = total
             return
-        final[k, rows] = total
+        partial[k, mine, rows] = total
         back_along[p, h].start()
 
     for p in (None, 0, 1, 2):
         k = 0 if p is None else order[p]
+        for way, side in ((1, pair_across), (0, pair)):
+            back_pairing[way, p] = remote(
+                partial.at[k, side],
+                paired.at[way, k],
+                rc_send.at[way, k],
+                rc_recv.at[way, k],
+                {"tp": pair},
+            )
         for h in range(2):
             rows = pl.ds(h * rows_half, rows_half)
             back_crossing[p, h] = remote(
-                leaving.at[k, rows],
+                partial.at[k, across, rows],
                 crossed.at[k, rows],
                 rx_send.at[k, h],
                 rx_recv.at[k, h],
@@ -685,7 +697,7 @@
             )
             if p is not None:
                 back_along[p, h] = remote(
-                    final.at[k, rows],
+                    partial.at[k, mine, rows],
                     returned.at[k, rows],
                     rz_send.at[k, h],
                     rz_recv.at[k, h],
@@ -700,7 +712,7 @@
     for h in range(2):
         block = slice(h * half, (h + 1) * half)
         mixer_copies[2 + h] = remote(
-            mleaving.at[block], mcrossed.at[block], m_send.at[2 + h], m_recv.at[2 + h], {"tp": across}
+            mixp.at[across, block], mcrossed.at[block], m_send.at[2 + h], m_recv.at[2 + h], {"tp": across}
         )
 
     def mixer_start():
@@ -725,7 +737,7 @@
 
         def add_tile(i, carry):
             rows = pl.ds(pl.multiple_of(h * half + i * step, step), step)
-            mleaving[rows, :] = (
+            mixp[across, rows, :] = (
                 mixp[across, rows, :].astype(jnp.float32) + mpaired[1, rows, :].astype(jnp.float32)
             ).astype(jnp.bfloat16)
             return carry
@@ -733,10 +745,16 @@
         lax.fori_loop(0, half // step, add_tile, 0)
         mixer_copies[2 + h].start()
 
+    outward = []
+    for i, (src, dst, size) in enumerate(((mix_ref, mix_hbm, half), (exp_ref, exp_hbm, span // 2))):
+        for h in range(2):
+            piece = pl.ds(h * size, size)
+            outward.append(
+                pltpu.make_async_copy(src.at[piece], dst.at[piece], out_sem.at[2 * i + h])
+            )
+
     def mixer_end():
         mixer_copies[0].wait_recv()
-        mixer_copies[2].wait_recv()
-        mixer_copies[3].wait_recv()
 
         def add_tile(i, carry):
             rows = rows_of(i, step)
@@ -748,7 +766,10 @@
             )
             return carry
 
-        lax.fori_loop(0, span // n_tp // step, add_tile, 0)
+        for h in range(2):
+            mixer_copies[2 + h].wait_recv()
+            lax.fori_loop(h * half // step, (h + 1) * half // step, add_tile, 0, unroll=2)
+            outward[h].start()
 
     outer = jnp.logical_not(inner)
     last = n_ep - 1
@@ -757,63 +778,113 @@
     only(me == 0, (mixer_start,))
     slot_tables(0, own)
     fill_slots(None, 0)
-    pass_on(0)
-    for k in range(1, n_ep):
+    split = exp_dev // 2
+    for copy in weights[: 3 * split]:
+        copy.wait()
+    expert_pass((None,), 0, 0, split)
+    pass_on(0, 0)
+    pass_on(0, 1)
+    for copy in weights[3 * split :]:
+        copy.wait()
+    expert_pass((None,), 0, split, exp_dev)
+    combine(None, 0)
+    notes_sent[0].wait_recv()
+    slot_tables(1, ranks(1))
+    only(inner, (pass_on, 1, 0), (pass_on, 1, 1))
+    back_cross(None, 0)
+    back_cross(None, 1)
+    for k in range(2, n_ep):
         notes_sent[k - 1].wait_recv()
         slot_tables(k, ranks(k))
-    only(inner, (kv_copies[0][1].start,))
-    for copy in weights:
-        copy.wait()
-    split = exp_dev // 2
-    expert_pass((None,), 0, 0, split)
-    relay(0)
-    only(inner, (pass_on, 1))
-    only(me == 0, (mixer_cross, 0))
-    expert_pass((None,), 0, split, exp_dev)
-    combine(None, 0)
-    fill_slots(0, 1)
-    back_cross(None, 0)
-    back_cross(None, 1)
-    only(me == 1, (kv_forward, 1))
-    only(inner, (pass_on, 2))
-    expert_pass((0,), 1, 0, split)
-    only(outer, (pass_on, 1))
-    only(inner, (relay, 1))
-    expert_pass((0,), 1, split, exp_dev)
-    combine(0, 1)
-    only(outer, (pass_on, 2))
-    only(me > 1, (kv_forward, 1))
-    only(inner, (back_cross, 0, 0), (back_cross, 0, 1))
-    only(me > 0, (attend, 1))
-    only(outer, (relay, 1))
-    only(inner, (relay, 2))
-    fill_slots(1, 0)
-    only(me == 0, (mixer_cross, 1))
-    only(me == 1, (mixer_start,))
-    only(me > 1, (kv_forward, 2), (attend, 2))
-    only(outer, (relay, 2), (back_cross, 0, 0), (back_cross, 0, 1))
-    only(me == 1, (mixer_cross, 0))
-    fill_slots(2, 1)
-    expert_pass((1, 2), 0, 0, split)
-    only(inner, (back_send, 0, 0), (back_send, 0, 1))
-    expert_pass((1, 2), 0, split, exp_dev)
-    only(outer, (back_send, 0, 0), (back_send, 0, 1))
-    combine(1, 0)
-    combine(2, 1)
-    back_cross(1, 0)
-    back_cross(1, 1)
-    only(me == 3, (kv_forward, 3), (attend, 3))
-    only(me > 1, (mixer_start,))
-    back_send(1, 0)
-    back_cross(2, 0)
-    back_send(1, 1)
-    back_cross(2, 1)
-    back_send(None, 0)
-    back_send(None, 1)
-    only(me > 1, (mixer_cross, 0))
-    back_send(2, 0)
-    back_send(2, 1)
-    only(me > 0, (mixer_cross, 1))
+    relay(0, 0)
+    relay(0, 1)
+
+    @pl.when(inner)
+    def _():
+        kv_copies[0][1].start()
+        fill_slots(0, 0)
+        pass_on(2, 0)
+        pass_on(2, 1)
+        only(me == 1, (kv_forward, 1), (attend, 1))
+        relay(1, 0)
+        relay(1, 1)
+        only(me == 1, (mixer_start,))
+        fill_slots(1, 1)
+        expert_pass((0, 1), 0, 0, split)
+        only(me == 2, (kv_forward, 1), (attend, 1))
+        relay(2, 0)
+        relay(2, 1)
+        only(me == 1, (mixer_cross, 0))
+        expert_pass((0, 1), 0, split, exp_dev)
+        combine(0, 0)
+        combine(1, 1)
+        only(me == 1, (back_cross, 0, 0), (back_cross, 0, 1))
+        only(me == 2, (back_cross, 1, 0), (back_cross, 1, 1), (kv_forward, 2))
+        fill_slots(2, 0)
+        expert_pass((2,), 0, 0, split)
+        only(me == 1, (back_cross, 1, 0), (back_cross, 1, 1), (back_send, 0, 0), (back_send, 0, 1))
+        only(me == 2, (back_cross, 0, 0), (back_cross, 0, 1), (back_send, 1, 0), (back_send, 1, 1))
+        expert_pass((2,), 0, split, exp_dev)
+        combine(2, 0)
+        only(me == 1, (back_send, 1, 0), (back_send, 1, 1))
+        only(me == 2, (back_send, 0, 0), (back_send, 0, 1))
+        back_cross(2, 0)
+        back_cross(2, 1)
+        only(me == 2, (attend, 2), (mixer_start,))
+        back_send(None, 0)
+        back_send(None, 1)
+        only(me == 1, (mixer_cross, 1))
+        back_send(2, 0)
+        only(me == 2, (mixer_cross, 0))
+        back_send(2, 1)
+        only(me == 2, (mixer_cross, 1))
+
+    @pl.when(outer)
+    def _():
+        fill_slots(0, 1)
+        step_of = exp_dev // 4
+        only(me == 0, (pass_on, 1, 0))
+        expert_pass((0,), 1, 0, 2 * step_of)
+        only(me == 0, (pass_on, 1, 1))
+        only(me == 3, (pass_on, 1, 0))
+        expert_pass((0,), 1, 2 * step_of, 3 * step_of)
+        only(me == 0, (pass_on, 2, 0))
+        only(me == 3, (pass_on, 1, 1))
+        expert_pass((0,), 1, 3 * step_of, exp_dev)
+        only(me == 3, (pass_on, 2, 0))
+        combine(0, 1)
+        pass_on(2, 1)
+        only(me == 3, (kv_forward, 1), (attend, 1))
+        relay(1, 0)
+        relay(1, 1)
+        fill_slots(1, 0)
+        relay(2, 0)
+        relay(2, 1)
+        back_cross(0, 0)
+        back_cross(0, 1)
+        only(me == 0, (mixer_cross, 0))
+        fill_slots(2, 1)
+        expert_pass((1, 2), 0, 0, exp_dev)
+        combine(1, 0)
+        back_send(0, 0)
+        back_send(0, 1)
+        combine(2, 1)
+        back_cross(1, 0)
+        back_cross(1, 1)
+        only(me == 3, (kv_forward, 2), (attend, 2), (kv_forward, 3), (attend, 3))
+        back_send(1, 0)
+        back_cross(2, 0)
+        back_send(1, 1)
+        back_cross(2, 1)
+        back_send(None, 0)
+        back_send(None, 1)
+        only(me == 0, (mixer_cross, 1))
+        only(me == 3, (mixer_start,))
+        back_send(2, 0)
+        only(me == 3, (mixer_cross, 0))
+        back_send(2, 1)
+        only(me == 3, (mixer_cross, 1))
+
     token_column = jnp.transpose(jnp.broadcast_to(token_key, (8, span)), (1, 0))[:, 0:1]
     for k in range(n_ep):
         base = ((me + k) % n_ep * row_cap).astype(jnp.float32)
@@ -822,6 +893,8 @@
         )
     for p in (None, 0, 1, 2):
         k = 0 if p is None else order[p]
+        if p == 2:
+            only(me < 2, (mixer_end,))
         if p is not None:
             for h in range(2):
                 back_along[p, h].wait_recv()
@@ -831,17 +904,24 @@
             total = dot_nn(final_hot[k, rows, :], returned[k])
             if p is not None:
                 total = total + exp_acc[rows, :]
-            if p == n_ep - 2:
+            if p == 2:
                 exp_ref[rows, :] = total.astype(jnp.bfloat16)
             else:
                 exp_acc[rows, :] = total
             return carry
 
-        lax.fori_loop(0, span // 128, output_tile, 0, unroll=2)
-    mixer_end()
+        if p == 2:
+            for h in range(2):
+                lax.fori_loop(h * span // 256, (h + 1) * span // 256, output_tile, 0, unroll=2)
+                outward[2 + h].start()
+        else:
+            lax.fori_loop(0, span // 128, output_tile, 0, unroll=2)
+    only(me > 1, (mixer_end,))
 
     for copy in notes_sent:
         copy.wait_send()
+    for copy in outward:
+        copy.wait()
     for d in range(n_ep - 1):
 
         @pl.when((me >= d) & (me < n_ep - 1))
@@ -849,7 +929,7 @@
             for copy in kv_copies[d]:
                 copy.wait_send()
 
-    for copy in along + crossing + pairing[0] + pairing[1] + pairing[2]:
+    for copy in along + crossing + sum(pairing, []):
         copy.wait_send()
     for group in (back_pairing, back_crossing, back_along, mixer_copies):
         for copy in group.values():
@@ -889,6 +969,8 @@
     vmem = pltpu.VMEM
     dma = pltpu.SemaphoreType.DMA
     scratch = [
+        vmem((span // n_tp, width), low),
+        vmem((span, quarter), low),
         vmem((span, heads * HEAD_SIZE), low),
         vmem((span, HEAD_SIZE), low),
         vmem((n_ep, 2, span, HEAD_SIZE), low),
@@ -896,7 +978,7 @@
         vmem((1, HEAD_SIZE), full),
         vmem((heads, whole), full),
         vmem((heads * HEAD_SIZE, width), low),
-        vmem((span, width), low),
+        vmem((n_tp, span // n_tp, width), low),
         vmem((1, width), full),
         vmem((TOP, span), jnp.int32),
         vmem((TOP, span), full),
@@ -909,9 +991,7 @@
         vmem((heads, span, 1), full),
         vmem((heads, span, HEAD_SIZE), full),
         vmem((span, heads * HEAD_SIZE), low),
-        vmem((n_tp, span // n_tp, width), low),
         vmem((2, span // n_tp, width), low),
-        vmem((span // n_tp, width), low),
         vmem((span // n_tp, width), low),
         vmem((span, width), low),
         vmem((span, span), low),
@@ -928,26 +1008,25 @@
         vmem((2, n_ep, row_cap, quarter), low),
         vmem((n_ep, row_cap, quarter), low),
         vmem((n_ep, row_cap, quarter), low),
-        vmem((n_ep, row_cap, quarter), low),
-        vmem((n_ep, row_cap, quarter), low),
-        dma((11,)),
+        dma((14,)),
         dma((3, exp_dev)),
         dma((n_ep, 2)),
         dma((n_ep, 2)),
         dma((n_ep,)),
         dma((n_ep,)),
-        dma((n_ep,)),
-        dma((n_ep,)),
-        dma((n_ep,)),
-        dma((n_ep,)),
-        dma((2, n_ep)),
-        dma((2, n_ep)),
+        dma((n_ep, 2)),
+        dma((n_ep, 2)),
+        dma((n_ep, 2)),
+        dma((n_ep, 2)),
+        dma((2, n_ep, 2)),
+        dma((2, n_ep, 2)),
         dma((2, n_ep)),
         dma((2, n_ep)),
         dma((n_ep, 2)),
         dma((n_ep, 2)),
         dma((n_ep, 2)),
         dma((n_ep, 2)),
+        dma((4,)),
         dma((4,)),
         dma((4,)),
     ]
@@ -959,8 +1038,8 @@
         ),
         in_specs=[pl.BlockSpec(memory_space=pl.ANY)] * 14,
         out_specs=(
-            pl.BlockSpec(memory_space=pltpu.VMEM),
-            pl.BlockSpec(memory_space=pltpu.VMEM),
+            pl.BlockSpec(memory_space=pltpu.HBM),
+            pl.BlockSpec(memory_space=pltpu.HBM),
         ),
         scratch_shapes=scratch,
         compiler_params=pltpu.CompilerParams(

time: 76.9 us -> 71.8 us (0.934)
  Pallas kernels: 75.9 us -> 70.8 us
    pallas_call x1, Pallas kernels: 73.9 us -> 68.8 us  [fused_half(): pl.pallas_call(functools.partial(fused_kernel, n_ep, n_tp, capacity), out...]
where the time goes in v3:
time: 71.8 us; the launch traced here: 71.6 us
  Pallas kernels  70.8 us (99%)
  between operations  0.82 us (1%)
    pallas_call x1, Pallas kernels, fused_half(): pl.pallas_call(functools.partial(fused_kernel, n_ep, n_tp, capacity), out...  68.8 us
    pallas_call x1, Pallas kernels, settle(): pl.pallas_call(settle_kernel, out_shape=tuple((jax.ShapeDtypeStruct(a.sha...  1.98 us

profile of v3, /device:TPU:0, one launch (start us, length us, event | category | flops | bytes accessed | tf_op | source)
XLA Modules:
  0.0 71.6 jit_solution(9376751799935375093)
XLA Ops:
  0.6 68.8 %shard_map.149 = (bf16[128,2048]{1,0:T(8,128)(2,1)}, bf16[512,512]{1,0:T(8,128)(2,1)}) custom-call(bf16[512,256]{1,0:T(8,128)(2,1)} %q_hbm.1, bf16[512,128]{1,0:T(8,128)(2,1)} %k_hbm.1, bf16[512,128]{1,0:T(8,128)(2,1)} %v_hbm.1, f32[1,128]{1,0:T(1,128)} %bitcast.4, f32[1,128]{1,0:T(1,128)} %bitcast.5, f32[2,2048]{1,0:T(2,128)} %lf_hbm.1, ...), custom_call_target="tpu_custom_call" | custom-call | tf_op jit(solution)/shard_map/pallas_call | solution.py:1033
  69.5 2.0 %shard_map.150 = (bf16[128,2048]{1,0:T(8,128)(2,1)}, bf16[512,512]{1,0:T(8,128)(2,1)}) custom-call(bf16[128,2048]{1,0:T(8,128)(2,1)} %get-tuple-element.4.first_in, bf16[512,512]{1,0:T(8,128)(2,1)} %get-tuple-element.5.second_in), custom_call_target="tpu_custom_call" | custom-call | tf_op jit(solution)/shard_map/pallas_call | solution.py:1089

commit v4 on v3

--- a/solution.py
+++ b/solution.py
@@ -791,8 +791,7 @@
     notes_sent[0].wait_recv()
     slot_tables(1, ranks(1))
     only(inner, (pass_on, 1, 0), (pass_on, 1, 1))
-    back_cross(None, 0)
-    back_cross(None, 1)
+    only(outer, (back_cross, None, 0), (back_cross, None, 1))
     for k in range(2, n_ep):
         notes_sent[k - 1].wait_recv()
         slot_tables(k, ranks(k))
@@ -811,18 +810,21 @@
         only(me == 1, (mixer_start,))
         fill_slots(1, 1)
         expert_pass((0, 1), 0, 0, split)
-        only(me == 2, (kv_forward, 1), (attend, 1))
         relay(2, 0)
         relay(2, 1)
+        only(me == 2, (back_cross, None, 0), (back_cross, None, 1))
         only(me == 1, (mixer_cross, 0))
         expert_pass((0, 1), 0, split, exp_dev)
+        only(me == 2, (kv_forward, 1))
         combine(0, 0)
         combine(1, 1)
         only(me == 1, (back_cross, 0, 0), (back_cross, 0, 1))
-        only(me == 2, (back_cross, 1, 0), (back_cross, 1, 1), (kv_forward, 2))
+        only(me == 2, (back_cross, 1, 0), (back_cross, 1, 1))
         fill_slots(2, 0)
         expert_pass((2,), 0, 0, split)
         only(me == 1, (back_cross, 1, 0), (back_cross, 1, 1), (back_send, 0, 0), (back_send, 0, 1))
+        only(me == 1, (back_cross, None, 0), (back_cross, None, 1))
+        only(me == 2, (kv_forward, 2))
         only(me == 2, (back_cross, 0, 0), (back_cross, 0, 1), (back_send, 1, 0), (back_send, 1, 1))
         expert_pass((2,), 0, split, exp_dev)
         combine(2, 0)
@@ -830,7 +832,7 @@
         only(me == 2, (back_send, 0, 0), (back_send, 0, 1))
         back_cross(2, 0)
         back_cross(2, 1)
-        only(me == 2, (attend, 2), (mixer_start,))
+        only(me == 2, (attend, 1), (attend, 2), (mixer_start,))
         back_send(None, 0)
         back_send(None, 1)
         only(me == 1, (mixer_cross, 1))
@@ -891,6 +893,20 @@
         final_hot[k] = one_hot(
             iota_f32((span, row_cap), 1) + base == token_column
         )
+    for copy in notes_sent:
+        copy.wait_send()
+    for d in range(n_ep - 1):
+
+        @pl.when((me >= d) & (me < n_ep - 1))
+        def _():
+            for copy in kv_copies[d]:
+                copy.wait_send()
+
+    for copy in along + crossing + sum(pairing, []):
+        copy.wait_send()
+    for copy in back_pairing.values():
+        copy.wait_send()
+
     for p in (None, 0, 1, 2):
         k = 0 if p is None else order[p]
         if p == 2:
@@ -918,20 +934,9 @@
             lax.fori_loop(0, span // 128, output_tile, 0, unroll=2)
     only(me > 1, (mixer_end,))
 
-    for copy in notes_sent:
-        copy.wait_send()
     for copy in outward:
         copy.wait()
-    for d in range(n_ep - 1):
-
-        @pl.when((me >= d) & (me < n_ep - 1))
-        def _():
-            for copy in kv_copies[d]:
-                copy.wait_send()
-
-    for copy in along + crossing + sum(pairing, []):
-        copy.wait_send()
-    for group in (back_pairing, back_crossing, back_along, mixer_copies):
+    for group in (back_crossing, back_along, mixer_copies):
         for copy in group.values():
             copy.wait_send()
 

time: 71.8 us -> 71 us (0.989)
  Pallas kernels: 70.8 us -> 69.7 us
    pallas_call x1, Pallas kernels: 68.8 us -> 67.7 us  [fused_half(): pl.pallas_call(functools.partial(fused_kernel, n_ep, n_tp, capacity), out...]
where the time goes in v4:
time: 71 us; the launch traced here: 70.5 us
  Pallas kernels  69.7 us (98%)
  between operations  0.82 us (1%)
    pallas_call x1, Pallas kernels, fused_half(): pl.pallas_call(functools.partial(fused_kernel, n_ep, n_tp, capacity), out...  67.7 us
    pallas_call x1, Pallas kernels, settle(): pl.pallas_call(settle_kernel, out_shape=tuple((jax.ShapeDtypeStruct(a.sha...  1.98 us

profile of v4, /device:TPU:0, one launch (start us, length us, event | category | flops | bytes accessed | tf_op | source)
XLA Modules:
  0.0 70.5 jit_solution(8477071214316541390)
XLA Ops:
  0.6 67.7 %shard_map.149 = (bf16[128,2048]{1,0:T(8,128)(2,1)}, bf16[512,512]{1,0:T(8,128)(2,1)}) custom-call(bf16[512,256]{1,0:T(8,128)(2,1)} %q_hbm.1, bf16[512,128]{1,0:T(8,128)(2,1)} %k_hbm.1, bf16[512,128]{1,0:T(8,128)(2,1)} %v_hbm.1, f32[1,128]{1,0:T(1,128)} %bitcast.4, f32[1,128]{1,0:T(1,128)} %bitcast.5, f32[2,2048]{1,0:T(2,128)} %lf_hbm.1, ...), custom_call_target="tpu_custom_call" | custom-call | tf_op jit(solution)/shard_map/pallas_call | solution.py:1038
  68.4 2.0 %shard_map.150 = (bf16[128,2048]{1,0:T(8,128)(2,1)}, bf16[512,512]{1,0:T(8,128)(2,1)}) custom-call(bf16[128,2048]{1,0:T(8,128)(2,1)} %get-tuple-element.4.first_in, bf16[512,512]{1,0:T(8,128)(2,1)} %get-tuple-element.5.second_in), custom_call_target="tpu_custom_call" | custom-call | tf_op jit(solution)/shard_map/pallas_call | solution.py:1094
